TPU v7x, 512 devices: a whole 4x8x8 slice. The times are simulated.
512 devices in a mesh: sp: 32 (over z, x), tp: 16 (over y, core).
Axes of the slice: x: 4, y: 8, z: 8, core: 2. Of those that a mesh axis runs over, the one named last changes fastest.
Arguments:
- moe_input: bfloat16 [6144, 2048], P('sp'), may hold values from -6 to 6
- out_grad: bfloat16 [6144, 2048], P('sp', 'tp'), may hold values from -6 to 6
- expert_ids: int32 [6144, 2], P('sp'), may hold values from 0 to 31, all different within a row; in each aligned block of 192 rows (0 to 191, 192 to 383, ...) at most 15 rows name the same one
- expert_weights: float32 [6144, 2], P('sp'), may hold values from 0.1 to 0.9
- w_gate: bfloat16 [32, 2048, 2048], P('sp', None, 'tp'), may hold values from -0.125 to 0.125
- w_up: bfloat16 [32, 2048, 2048], P('sp', None, 'tp'), may hold values from -0.125 to 0.125
- w_down: bfloat16 [32, 2048, 2048], P('sp', 'tp'), may hold values from -0.125 to 0.125
- out_proj: bfloat16 [1536, 2048], P('tp'), may hold values from -0.15625 to 0.15625
- retained: bfloat16 [6144, 1536], P('sp', 'tp'), may hold values from -6 to 6
- queries: bfloat16 [6144, 768], P('sp', 'tp'), may hold values from -6 to 6
- keys: bfloat16 [6144, 768], P('sp', 'tp'), may hold values from -0.86328125 to 0.86328125
- values: bfloat16 [6144, 1536], P('sp', 'tp'), may hold values from -6 to 6
- log_decay: float32 [6144, 16], P('sp', 'tp'), may hold values from -1 to 0
- incoming_state: float32 [32, 16, 48, 96], P('sp', 'tp'), may hold values from -6 to 6
Outputs:
- w_gate_grad: bfloat16 [32, 2048, 2048], P('sp', None, 'tp')
- w_up_grad: bfloat16 [32, 2048, 2048], P('sp', None, 'tp')
- w_down_grad: bfloat16 [32, 2048, 2048], P('sp', 'tp')
- out_proj_grad: float32 [2048, 1536], P('sp', 'tp')
- query_grad: bfloat16 [6144, 768], P('sp', 'tp')
- key_grad: bfloat16 [6144, 768], P('sp', 'tp')
- value_grad: bfloat16 [6144, 1536], P('sp', 'tp')
Inputs may be any that keep to these rules, and one draw needn't show every extreme that they name: `expert_ids`: in each aligned block of 192 positions no expert is named by more than 15 of the block's assignments, a bound that some block reaches.
All inputs are finite; a program needn't handle non-finite values.
Results may differ from a plain program's by a relative error of at most 0.02.
Values may be sent and summed in bfloat16 or wider, within the bound.
No kernel may reach another device: no remote copies, remote signals or barrier semaphores. Data moves between devices by JAX's collectives and lax.ppermute only.
A program may use at most 64 MiB of HBM per device.

v0:
```python
import jax
import jax.numpy as jnp
from jax import lax
from jax.sharding import Mesh
from jax.sharding import PartitionSpec as P

TP = ("tp_0", "tp_1")


def sent_together(arrays, axis, split_dim, concat_dim, along):
    widths = [a.shape[along] for a in arrays]
    both = jnp.concatenate(arrays, axis=along)
    whole = lax.all_to_all(both, axis, split_axis=split_dim, concat_axis=concat_dim, tiled=True)
    return tuple(jnp.split(whole, [sum(widths[:k]) for k in range(1, len(widths))], axis=along))


def sent_together_2(arrays, axis, dim, along):
    both = jnp.concatenate(arrays, axis=along)
    whole, at, outs = (lax.all_gather(both, axis, axis=dim, tiled=True), 0, [])
    for a in arrays:
        outs.append(lax.slice_in_dim(whole, at, at + a.shape[along], axis=along))
        at += a.shape[along]
    return tuple(outs)


def split_up(x, dim, devices):
    dims = x.shape
    pieces = x.reshape(*dims[:dim], devices, dims[dim] // devices, *dims[dim + 1 :])
    return jnp.moveaxis(pieces, dim, 0)


def sent_and_summed(x, axis, dim):
    devices = lax.axis_size(axis)
    pieces = lax.all_to_all(split_up(x, dim, devices), axis, 0, 0, tiled=True)
    return jnp.sum(pieces.astype(jnp.float32), axis=0)


def gather_axes(x, axes, dim):
    if not axes:
        return x
    nearer = lax.all_gather(x, axes[-1], axis=dim, tiled=True)
    return gather_axes(nearer, axes[:-1], dim)


def copy_for_each(x, axis):
    devices = lax.axis_size(axis)
    return lax.all_to_all(jnp.broadcast_to(x[None], (devices, *x.shape)), axis, 0, 0, tiled=True)


def all_in_one(x, axis):
    leaves = jax.tree.leaves(x)
    order = sorted(range(len(leaves)), key=lambda k: -leaves[k].size)
    width = (1, *leaves[order[0]].shape)[-1]
    lines = [
        jnp.pad(leaves[k].reshape(-1), (0, -leaves[k].size % width)).reshape(-1, width)
        for k in order
    ]
    both, at, found = (copy_for_each(jnp.concatenate(lines), axis), 0, {})
    for k, line in zip(order, lines):
        slab = both[:, at : at + len(line)].reshape(len(both), -1)
        found[k] = slab[:, : leaves[k].size].reshape(-1, *leaves[k].shape)
        at += len(line)
    numbers = iter(range(len(leaves)))
    return jax.tree.map(lambda _: found[next(numbers)], x)


def folded_in_pairs(pieces, combine):
    while len(jax.tree.leaves(pieces)[0]) > 1:
        pieces = jax.vmap(combine)(
            *(jax.tree.map(lambda part: part[side::2], pieces) for side in (0, 1))
        )
    return jax.tree.map(lambda part: part[0], pieces)


def carried_in(x, axis, combine, identity):
    devices, place = (lax.axis_size(axis), lax.axis_index(axis))
    passed = jnp.arange(devices) > place

    def kept(part, zero, own):
        part = jnp.where(
            passed.reshape(-1, *(1 for _ in own.shape)), part, jnp.asarray(zero, own.dtype)
        )
        return part[::-1]

    pieces = all_in_one(x, axis)
    return folded_in_pairs(jax.tree.map(kept, pieces, identity, x), combine)


def expert_back(rows, grad, gate_w, up_w, down_w):
    f32 = jnp.float32
    bf16 = jnp.bfloat16
    gate = jnp.dot(rows, gate_w, preferred_element_type=f32)
    up = jnp.dot(rows, up_w, preferred_element_type=f32)
    sig = jax.nn.sigmoid(gate)
    swish = gate * sig
    act = (swish * up).astype(bf16)
    across = (((1,), (1,)), ((), ()))
    along = (((0,), (0,)), ((), ()))
    act_grad = lax.dot_general(grad, down_w, across, preferred_element_type=f32)
    gate_grad = (act_grad * up * sig * (1.0 + gate * (1.0 - sig))).astype(bf16)
    up_grad = (act_grad * swish).astype(bf16)
    down_grad = lax.dot_general(act, grad, along, preferred_element_type=f32).astype(bf16)
    gate_w_grad = lax.dot_general(rows, gate_grad, along, preferred_element_type=f32).astype(bf16)
    up_w_grad = lax.dot_general(rows, up_grad, along, preferred_element_type=f32).astype(bf16)
    partial_value = lax.dot_general(
        gate_grad, gate_w, across, preferred_element_type=f32
    ) + lax.dot_general(up_grad, up_w, across, preferred_element_type=f32)
    return (gate_w_grad, up_w_grad, down_grad, partial_value)


def combine_states(earlier, later):
    return (later[0] * earlier[0], later[1] + later[0][:, None, None] * earlier[1])


def on_device(
    moe_input,
    out_grad,
    expert_ids,
    expert_weights,
    w_gate,
    w_up,
    w_down,
    out_proj,
    retained,
    queries,
    keys,
    values,
    log_decay,
    incoming_state,
):
    f32 = jnp.float32
    bf16 = jnp.bfloat16
    tokens_here = moe_input.shape[0]
    width = moe_input.shape[1]
    sp_count = lax.axis_size("sp")
    tp_count = lax.axis_size(TP)
    capacity = 5 * tokens_here // (2 * sp_count)
    slot_count = sp_count * capacity
    flat_ids = expert_ids.reshape(-1)
    flat_weights = expert_weights.reshape(-1)
    onehot = (flat_ids[:, None] == jnp.arange(sp_count, dtype=jnp.int32)[None, :]).astype(jnp.int32)
    ranks = jnp.sum((jnp.cumsum(onehot, axis=0) - onehot) * onehot, axis=1)
    slot_of = flat_ids * capacity + ranks
    hits = jnp.arange(slot_count, dtype=jnp.int32)[:, None] == slot_of[None, :]
    picker = jnp.any(hits.reshape(slot_count, tokens_here, 2), axis=2).astype(bf16)
    slot_weight = jnp.sum(jnp.where(hits, flat_weights[None, :], 0.0), axis=1)
    along = (((0,), (0,)), ((), ()))
    column_count = width // tp_count
    own_rows = lax.dynamic_slice_in_dim(
        moe_input, lax.axis_index(TP) * column_count, column_count, 1
    )
    send_rows = jnp.dot(picker, own_rows, preferred_element_type=f32).astype(bf16)
    send_grad = (
        jnp.dot(picker, out_grad, preferred_element_type=f32) * slot_weight[:, None]
    ).astype(bf16)
    part_rows, part_grad = sent_together((send_rows, send_grad), "sp", 0, 0, 1)
    recv_rows, recv_grad = sent_together_2((part_rows, part_grad), TP, 1, 0)
    gate_w_grad, up_w_grad, down_grad, partial_value = expert_back(
        recv_rows, recv_grad, w_gate[0], w_up[0], w_down[0]
    )
    share = sent_and_summed(partial_value.astype(jnp.bfloat16), TP, 1).astype(bf16)
    returned = lax.all_to_all(share, "sp", split_axis=0, concat_axis=0, tiled=True)
    token_grad = lax.dot_general(picker, returned, along, preferred_element_type=f32)
    stream_part = (out_grad.astype(f32) + token_grad).astype(bf16)
    stream = gather_axes(stream_part, TP, 1)
    ret_grad = lax.dot_general(
        stream, out_proj, (((1,), (1,)), ((), ())), preferred_element_type=f32
    ).astype(bf16)
    out_proj_grad = sent_and_summed(
        lax.dot_general(stream, retained, along, preferred_element_type=f32).astype(jnp.bfloat16),
        "sp",
        0,
    )
    heads_here = log_decay.shape[1]
    key_dim = queries.shape[1] // heads_here
    value_dim = values.shape[1] // heads_here
    query_rows = queries.astype(f32).reshape(tokens_here, heads_here, key_dim)
    key_matrix = keys.astype(f32).reshape(tokens_here, heads_here, key_dim)
    value_matrix = values.astype(f32).reshape(tokens_here, heads_here, value_dim)
    incoming_gradient = ret_grad.astype(f32).reshape(tokens_here, heads_here, value_dim)
    running_total = jnp.cumsum(log_decay, axis=0)
    last_sum = running_total[-1]
    place = jnp.arange(tokens_here)
    causal = (place[:, None] >= place[None, :])[:, :, None]
    diff = running_total[:, None, :] - running_total[None, :, :]
    decay = jnp.where(causal, jnp.exp(jnp.minimum(diff, 0.0)), 0.0)
    scores = jnp.einsum("thk,shk->tsh", query_rows, key_matrix) * decay
    prob_grad = jnp.einsum("thv,shv->tsh", incoming_gradient, value_matrix) * decay
    added_input = jnp.einsum(
        "yb,ybm,ybx->bmx", jnp.exp(running_total), query_rows, incoming_gradient
    )
    block_multiplier = jnp.exp(last_sum)
    _, state_gradient = carried_in(
        (block_multiplier, added_input),
        "sp",
        combine_states,
        (jnp.ones_like(block_multiplier), jnp.zeros_like(added_input)),
    )
    tail = jnp.exp(last_sum[None, :] - running_total)[..., None]
    query_grad = jnp.einsum("tsh,shk->thk", prob_grad, key_matrix) + jnp.exp(running_total)[
        ..., None
    ] * jnp.einsum("ybc,bfc->ybf", incoming_gradient, incoming_state[0])
    key_grad = jnp.einsum("tsh,thk->shk", prob_grad, query_rows) + tail * jnp.einsum(
        "rgd,gnd->rgn", value_matrix, state_gradient
    )
    value_grad = jnp.einsum("tsh,thv->shv", scores, incoming_gradient) + tail * jnp.einsum(
        "bgi,gie->bge", key_matrix, state_gradient
    )
    return (
        gate_w_grad[None],
        up_w_grad[None],
        down_grad[None],
        out_proj_grad,
        query_grad.reshape(tokens_here, -1).astype(bf16),
        key_grad.reshape(tokens_here, -1).astype(bf16),
        value_grad.reshape(tokens_here, -1).astype(bf16),
    )


def solution(mesh):
    torus = Mesh(mesh.devices.reshape(mesh.shape["sp"], 8, 2), ("sp", "tp_0", "tp_1"))
    placed = (
        P("sp", None),
        P("sp", TP),
        P("sp", None),
        P("sp", None),
        P("sp", None, TP),
        P("sp", None, TP),
        P("sp", TP, None),
        P(TP, None),
        P("sp", TP),
        P("sp", TP),
        P("sp", TP),
        P("sp", TP),
        P("sp", TP),
        P("sp", TP, None, None),
    )
    return jax.shard_map(
        on_device,
        mesh=torus,
        in_specs=placed,
        out_specs=(
            P("sp", None, TP),
            P("sp", None, TP),
            P("sp", TP, None),
            P("sp", TP),
            P("sp", TP),
            P("sp", TP),
            P("sp", TP),
        ),
        check_vma=False,
    )
```

profile of v0, /device:TPU:4, one launch (start us, length us, event | category | flops | bytes accessed | tf_op | source)
XLA Modules:
  0.0 253.7 jit_solution(18360480132314000063)
XLA Ops:
  7.2 0.9 copy.63
  8.4 0.9 reduce-window.14
  9.9 0.7 multiply_add_fusion.5
  10.8 0.8 copy.67
  12.0 1.1 fusion.13
  13.6 24.4 %all_to_all.39 = bf16[32,15,256]{2,1,0:T(8,128)(2,1)S(1)} all-to-all(bf16[32,15,256]{2,1,0:T(8,128)(2,1)S(1)} %all_to_all.25), channel_id=1, replica_groups=mesh['sp'=32,'tp_0'=8,'tp_1'=2] {'sp'}, dimensions={0} | all-to-all | bytes 491520 | tf_op jit(solution)/shard_map/all_to_all | solution.py:13
  38.9 47.4 %all-gather.2.cloned.1.call-done = bf16[960,2048]{1,0:T(8,128)(2,1)} async-done(((bf16[960,128]{1,0:T(8,128)(2,1)}), bf16[960,2048]{1,0:T(8,128)(2,1)}) %all-gather.2.cloned.1.call-update) | async-done | bytes 3932176 | tf_op jit(solution)/shard_map/all_gather | solution.py:19
  86.3 2.4 fusion.9
  88.7 2.3 fusion.11
  93.1 1.6 copy.77
  94.8 4.3 %all-to-all-start.1 = ((bf16[16,480,128]{2,1,0:T(8,128)(2,1)}), bf16[16,480,128]{2,1,0:T(8,128)(2,1)S(1)}, u32[]{:S(2)}, u32[]{:S(2)}) async-start(bf16[16,480,128]{2,1,0:T(8,128)(2,1)} %bitcast.189), calls=%async_computation.1 | async-start | bytes 3932160 | tf_op jit(solution)/shard_map/all_to_all | solution.py:34
  99.8 45.7 %all-to-all-done.1 = bf16[16,480,128]{2,1,0:T(8,128)(2,1)S(1)} async-done(((bf16[16,480,128]{2,1,0:T(8,128)(2,1)}), bf16[16,480,128]{2,1,0:T(8,128)(2,1)S(1)}, u32[]{:S(2)}, u32[]{:S(2)}) %all-to-all-start.1) | async-done | bytes 1966112 | tf_op jit(solution)/shard_map/all_to_all | solution.py:34
  146.4 10.5 %all-to-all-start.2 = ((bf16[32,15,128]{2,1,0:T(8,128)(2,1)}), bf16[32,15,128]{2,1,0:T(8,128)(2,1)S(1)}, u32[]{:S(2)}, u32[]{:S(2)}) async-start(bf16[32,15,128]{2,1,0:T(8,128)(2,1)} %all_to_all.29), calls=%async_computation.2 | async-start | bytes 262144 | tf_op jit(solution)/shard_map/all_to_all | solution.py:162
  158.9 7.0 %all-to-all-done.2 = bf16[32,15,128]{2,1,0:T(8,128)(2,1)S(1)} async-done(((bf16[32,15,128]{2,1,0:T(8,128)(2,1)}), bf16[32,15,128]{2,1,0:T(8,128)(2,1)S(1)}, u32[]{:S(2)}, u32[]{:S(2)}) %all-to-all-start.2) | async-done | bytes 122912 | tf_op jit(solution)/shard_map/all_to_all | solution.py:162
  166.0 1.1 fusion.20
  167.1 1.9 all_gather.10
  169.0 26.2 %all_gather.11 = bf16[192,2048]{1,0:T(8,128)(2,1)S(1)} all-gather(bf16[192,256]{1,0:T(8,128)(2,1)S(1)} %all_gather.10), channel_id=1, replica_groups=mesh['sp'=32,'tp_0'=8,'tp_1'=2] {'tp_0'}, dimensions={1}, use_global_device_ids=true | all-gather | bytes 884736 | tf_op jit(solution)/shard_map/all_gather | solution.py:41
  195.2 1.1 convolution_convert_fusion.3
  196.3 1.0 copy.69
  197.3 5.7 %all-to-all-start.3 = ((bf16[32,64,96]{2,1,0:T(8,128)(2,1)}), bf16[32,64,96]{2,1,0:T(8,128)(2,1)S(1)}, u32[]{:S(2)}, u32[]{:S(2)}) async-start(bf16[32,64,96]{2,1,0:T(8,128)(2,1)} %bitcast.8), calls=%async_computation.3 | async-start | bytes 1048576 | tf_op jit(solution)/shard_map/all_to_all | solution.py:34
  203.6 12.1 %all-to-all-done.3 = bf16[32,64,96]{2,1,0:T(8,128)(2,1)S(1)} async-done(((bf16[32,64,96]{2,1,0:T(8,128)(2,1)}), bf16[32,64,96]{2,1,0:T(8,128)(2,1)S(1)}, u32[]{:S(2)}, u32[]{:S(2)}) %all-to-all-start.3) | async-done | bytes 393248 | tf_op jit(solution)/shard_map/all_to_all | solution.py:34
  215.7 1.0 broadcast_in_dim.71
  216.7 5.7 %all-to-all-start.4 = ((f32[32,49,96]{2,1,0:T(8,128)}), f32[32,49,96]{2,1,0:T(8,128)S(1)}, u32[]{:S(2)}, u32[]{:S(2)}) async-start(f32[32,49,96]{2,1,0:T(8,128)} %broadcast_in_dim.71), calls=%async_computation.4 | async-start | bytes 1835008 | tf_op jit(solution)/shard_map/all_to_all | solution.py:47
  222.4 3.3 %fusion = bf16[1,2048,128]{2,1,0:T(8,128)(2,1)} fusion(bf16[480,128]{1,0:T(8,128)(2,1)S(1)} %get-tuple-element.52, bf16[960,2048]{1,0:T(8,128)(2,1)} %all-gather.2.cloned.1.call-done), kind=kOutput, calls=%fused_computation.5 | convolution fusion | flops 251920384 | bytes 2613248 | tf_op jit(solution)/shard_map/dot_general | solution.py:103
  225.7 3.1 %fusion.1 = bf16[1,2048,128]{2,1,0:T(8,128)(2,1)} fusion(bf16[480,128]{1,0:T(8,128)(2,1)S(1)} %get-tuple-element.51, bf16[960,2048]{1,0:T(8,128)(2,1)} %all-gather.2.cloned.1.call-done), kind=kOutput, calls=%fused_computation.6 | convolution fusion | flops 251920384 | bytes 2613248 | tf_op jit(solution)/shard_map/dot_general | solution.py:104
  228.9 1.3 fusion.2
  230.5 0.8 fusion.30
  231.5 0.7 convert_reduce_fusion
  232.2 9.6 %all-to-all-done.4 = f32[32,49,96]{2,1,0:T(8,128)S(1)} async-done(((f32[32,49,96]{2,1,0:T(8,128)}), f32[32,49,96]{2,1,0:T(8,128)S(1)}, u32[]{:S(2)}, u32[]{:S(2)}) %all-to-all-start.4) | async-done | bytes 602144 | tf_op jit(solution)/shard_map/all_to_all | solution.py:47
  243.5 0.8 fusion.19
  244.4 1.4 fusion.29
  246.2 0.7 copy.71
  (101 shorter events, 10.8 us)
Async XLA Ops:
  7.2 6.0 %copy-start = (bf16[192,2048]{1,0:T(8,128)(2,1)S(1)}, bf16[192,2048]{1,0:T(8,128)(2,1)}, u32[]{:S(2)}) copy-start(bf16[192,2048]{1,0:T(8,128)(2,1)} %param.14) | copy-start | bytes 2359300
  7.2 79.1 %copy-start.1 = (bf16[1,2048,128]{2,1,0:T(8,128)(2,1)S(1)}, bf16[1,2048,128]{2,1,0:T(8,128)(2,1)}, u32[]{:S(2)}) copy-start(bf16[1,2048,128]{2,1,0:T(8,128)(2,1)} %param.18) | copy-start | bytes 1572868
  7.2 79.1 %all-gather.2.cloned.1.call-start = ((), (), s32[]{:S(2)}) async-start(), calls=%async_computation.5 | async-start | bytes 4177920 | tf_op jit(solution)/shard_map/all_gather | solution.py:19
  9.8 78.9 %copy-start.2 = (bf16[1,2048,128]{2,1,0:T(8,128)(2,1)S(1)}, bf16[1,2048,128]{2,1,0:T(8,128)(2,1)}, u32[]{:S(2)}) copy-start(bf16[1,2048,128]{2,1,0:T(8,128)(2,1)} %param.19) | copy-start | bytes 1572868
  10.8 2.7 %copy-start.4 = (pred[480,192]{0,1:T(8,128)(4,1)}, pred[480,192]{0,1:T(8,128)(4,1)S(1)}, u32[]{:S(2)}) copy-start(pred[480,192]{0,1:T(8,128)(4,1)S(1)} %fusion.32) | copy-start | bytes 276484
  38.2 52.8 %copy-start.12 = (bf16[1,128,2048]{2,1,0:T(8,128)(2,1)S(1)}, bf16[1,128,2048]{2,1,0:T(8,128)(2,1)}, u32[]{:S(2)}) copy-start(bf16[1,128,2048]{2,1,0:T(8,128)(2,1)} %param.20) | copy-start | bytes 1572868
  86.3 4.7 %copy-start.10 = (bf16[960,2048]{1,0:T(8,128)(2,1)S(1)}, bf16[960,2048]{1,0:T(8,128)(2,1)}, u32[]{:S(2)}) copy-start(bf16[960,2048]{1,0:T(8,128)(2,1)} %all-gather.2.cloned.1.call-done) | copy-start | bytes 11796484
  88.7 3.0 %copy-start.13 = (f32[480,128]{1,0:T(8,128)}, f32[480,128]{1,0:T(8,128)S(1)}, u32[]{:S(2)}) copy-start(f32[480,128]{1,0:T(8,128)S(1)} %fusion.9) | copy-start | bytes 737284
  91.0 1.4 copy-start.15
  93.1 6.0 %copy-start.9 = (f32[192,1]{0,1:T(1,128)S(1)}, f32[192,1]{0,1:T(1,128)}, u32[]{:S(2)}) copy-start(f32[192,1]{0,1:T(1,128)} %param.26) | copy-start | bytes 2308
  94.8 50.7 %all-to-all-start.1 = ((bf16[16,480,128]{2,1,0:T(8,128)(2,1)}), bf16[16,480,128]{2,1,0:T(8,128)(2,1)S(1)}, u32[]{:S(2)}, u32[]{:S(2)}) async-start(bf16[16,480,128]{2,1,0:T(8,128)(2,1)} %bitcast.189), calls=%async_computation.1 | async-start | bytes 3932160 | tf_op jit(solution)/shard_map/all_to_all | solution.py:34
  99.1 104.0 %copy-start.3 = (bf16[96,2048]{1,0:T(8,128)(2,1)S(1)}, bf16[96,2048]{1,0:T(8,128)(2,1)}, u32[]{:S(2)}) copy-start(bf16[96,2048]{1,0:T(8,128)(2,1)} %param.21) | copy-start | bytes 1179652
  99.8 103.6 %copy-start.6 = (bf16[192,48]{0,1:T(8,128)(2,1)S(1)}, bf16[192,48]{0,1:T(8,128)(2,1)}, u32[]{:S(2)}) copy-start(bf16[192,48]{0,1:T(8,128)(2,1)} %param.23) | copy-start | bytes 55300
  146.4 19.5 %all-to-all-start.2 = ((bf16[32,15,128]{2,1,0:T(8,128)(2,1)}), bf16[32,15,128]{2,1,0:T(8,128)(2,1)S(1)}, u32[]{:S(2)}, u32[]{:S(2)}) async-start(bf16[32,15,128]{2,1,0:T(8,128)(2,1)} %all_to_all.29), calls=%async_computation.2 | async-start | bytes 262144 | tf_op jit(solution)/shard_map/all_to_all | solution.py:162
  197.3 18.4 %all-to-all-start.3 = ((bf16[32,64,96]{2,1,0:T(8,128)(2,1)}), bf16[32,64,96]{2,1,0:T(8,128)(2,1)S(1)}, u32[]{:S(2)}, u32[]{:S(2)}) async-start(bf16[32,64,96]{2,1,0:T(8,128)(2,1)} %bitcast.8), calls=%async_computation.3 | async-start | bytes 1048576 | tf_op jit(solution)/shard_map/all_to_all | solution.py:34
  216.7 12.1 %copy-start.14 = (f32[480,128]{1,0:T(8,128)S(1)}, f32[480,128]{1,0:T(8,128)}, u32[]{:S(2)}) copy-start(f32[480,128]{1,0:T(8,128)} %copy-done.13) | copy-start | bytes 737284
  216.7 12.1 %copy-start.16 = (f32[480,128]{1,0:T(8,128)S(1)}, f32[480,128]{1,0:T(8,128)}, u32[]{:S(2)}) copy-start(f32[480,128]{1,0:T(8,128)} %copy-done.15) | copy-start | bytes 737284
  216.7 25.1 %all-to-all-start.4 = ((f32[32,49,96]{2,1,0:T(8,128)}), f32[32,49,96]{2,1,0:T(8,128)S(1)}, u32[]{:S(2)}, u32[]{:S(2)}) async-start(f32[32,49,96]{2,1,0:T(8,128)} %broadcast_in_dim.71), calls=%async_computation.4 | async-start | bytes 1835008 | tf_op jit(solution)/shard_map/all_to_all | solution.py:47
  222.4 6.5 %copy-start.11 = (bf16[960,2048]{1,0:T(8,128)(2,1)S(1)}, bf16[960,2048]{1,0:T(8,128)(2,1)}, u32[]{:S(2)}) copy-start(bf16[960,2048]{1,0:T(8,128)(2,1)} %all-gather.2.cloned.1.call-done) | copy-start | bytes 11796484
  225.7 4.5 %copy-start.7 = (bf16[192,96]{1,0:T(8,128)(2,1)S(1)}, bf16[192,96]{1,0:T(8,128)(2,1)}, u32[]{:S(2)}) copy-start(bf16[192,96]{1,0:T(8,128)(2,1)} %param.25) | copy-start | bytes 110596
  225.7 4.7 %copy-start.5 = (bf16[192,48]{0,1:T(8,128)(2,1)S(1)}, bf16[192,48]{0,1:T(8,128)(2,1)}, u32[]{:S(2)}) copy-start(bf16[192,48]{0,1:T(8,128)(2,1)} %param.24) | copy-start | bytes 55300
  225.7 4.8 %copy-start.8 = (f32[1,1,48,96]{3,2,1,0:T(8,128)S(1)}, f32[1,1,48,96]{3,2,1,0:T(8,128)}, u32[]{:S(2)}) copy-start(f32[1,1,48,96]{3,2,1,0:T(8,128)} %param.27) | copy-start | bytes 55300
Sparse Core Ops, SparseCore 0:
  39.1 47.2 all-gather.1
where the time goes:
time: 255 us; the launch traced here: 254 us
  waiting for transfers between devices  122 us (48%)
  blocking collectives  52.5 us (21%)
  starting transfers between devices  26.2 us (10%)
  matrix products  22.6 us (9%)
  between operations  15.2 us (6%)
  local copies, waits for them, and re-layouts  9.55 us (4%)
  other arithmetic  5.93 us (2%)
    all_to_all x2, waiting for transfers between devices, sent_and_summed(): pieces = lax.all_to_all(split_up(x, dim, devices), axis, 0, 0, tiled=True)  57.8 us
    all_gather x1, waiting for transfers between devices, sent_together_2(): whole, at, outs = (lax.all_gather(both, axis, axis=dim, tiled=True), 0, [])  47.4 us
    all_gather x2, blocking collectives, gather_axes(): nearer = lax.all_gather(x, axes[-1], axis=dim, tiled=True)  28.1 us
    all_to_all x1, blocking collectives, sent_together(): lax.all_to_all(both, axis, split_axis=split_dim, concat_axis=concat_dim,...  24.4 us
    all_to_all x1, starting transfers between devices, on_device(): lax.all_to_all(share, 'sp', split_axis=0, concat_axis=0, tiled=True)  10.5 us
    all_to_all x2, starting transfers between devices, sent_and_summed(): pieces = lax.all_to_all(split_up(x, dim, devices), axis, 0, 0, tiled=True)  9.96 us
    all_to_all x1, waiting for transfers between devices, copy_for_each(): lax.all_to_all(jnp.broadcast_to(x[None], (devices, *x.shape)), axis, 0, 0...  9.56 us
    all_to_all x1, waiting for transfers between devices, on_device(): lax.all_to_all(share, 'sp', split_axis=0, concat_axis=0, tiled=True)  7.02 us
  transfers between devices with their start and end apart: 5, of which 5 were waited for; matrix products, arithmetic and copies ran while one was open for 5% of the time, Pallas kernels for 0%

commit v1 on v0

v1 whole, which is shorter than its diff:
```python
import jax
import jax.numpy as jnp
from jax import lax
from jax.sharding import Mesh
from jax.sharding import PartitionSpec as P

TP = ("y", "c")
F32 = jnp.float32
BF16 = jnp.bfloat16
ACROSS = (((1,), (1,)), ((), ()))
ALONG = (((0,), (0,)), ((), ()))
SWAP = [(0, 1), (1, 0)]


def dot(a, b, dims=(((1,), (0,)), ((), ()))):
    return lax.dot_general(a, b, dims, preferred_element_type=F32)


def slot_tables(expert_ids, expert_weights, experts, capacity, padded):
    tokens = expert_ids.shape[0]
    ids = expert_ids.T
    weights = expert_weights.T
    names = jnp.arange(experts, dtype=jnp.int32)[:, None]
    onehot = [(names == ids[j][None, :]).astype(BF16) for j in (0, 1)]
    place = jnp.arange(tokens)
    earlier = (place[:, None] < place[None, :]).astype(BF16)
    before = dot(onehot[0] + onehot[1], earlier)
    slots = jnp.arange(experts * padded, dtype=jnp.int32)[:, None]
    picker, slot_weight = 0.0, 0.0
    for j in (0, 1):
        rank = jnp.sum(before * onehot[j].astype(F32), axis=0).astype(jnp.int32)
        hits = slots == (ids[j] * padded + rank)[None, :]
        picker = picker + jnp.where(hits, 1.0, 0.0)
        slot_weight = slot_weight + jnp.sum(
            jnp.where(hits, weights[j][None, :], 0.0), axis=1, keepdims=True
        )
    return picker.astype(BF16), slot_weight


def parity_columns(x, index):
    rows, cols = x.shape
    return lax.dynamic_index_in_dim(
        x.reshape(rows, 8, 2, cols // 16), index, 2, keepdims=False
    ).reshape(rows, cols // 2)


def parity_rows(x, index):
    rows, cols = x.shape
    return lax.dynamic_index_in_dim(
        x.reshape(8, 2, rows // 16, cols), index, 1, keepdims=False
    ).reshape(rows // 2, cols)


def joined_rows(own, other, core):
    rows, cols = own.shape
    own, other = (a.reshape(8, 1, rows // 8, cols) for a in (own, other))
    first = jnp.where(core == 0, own, other)
    second = jnp.where(core == 0, other, own)
    return jnp.concatenate([first, second], axis=1).reshape(2 * rows, cols)


def joined_columns(own, other, core):
    rows, cols = own.shape
    own, other = (a.reshape(rows, 8, 1, cols // 8) for a in (own, other))
    first = jnp.where(core == 0, own, other)
    second = jnp.where(core == 0, other, own)
    return jnp.concatenate([first, second], axis=2).reshape(rows, 2 * cols)


def in_three(x):
    high = x.astype(BF16)
    rest = x - high.astype(F32)
    middle = rest.astype(BF16)
    low = (rest - middle.astype(F32)).astype(BF16)
    return high, middle, low


def on_device(
    moe_input,
    out_grad,
    expert_ids,
    expert_weights,
    w_gate,
    w_up,
    w_down,
    out_proj,
    retained,
    queries,
    keys,
    values,
    log_decay,
    incoming_state,
):
    tokens = moe_input.shape[0]
    width = moe_input.shape[1]
    sp_count = lax.axis_size("sp")
    capacity = 5 * tokens // (2 * sp_count)
    padded = 16
    slot_count = sp_count * capacity
    core = lax.axis_index("c")
    block = lax.axis_index("sp")
    chunk = out_grad.shape[1]

    running = jnp.cumsum(log_decay[:, 0])
    last = running[-1]

    picker, slot_weight = slot_tables(expert_ids, expert_weights, sp_count, capacity, padded)
    mine = parity_columns(moe_input, core)
    send_rows = dot(picker, mine).astype(BF16).reshape(sp_count, padded, -1)
    parts = in_three(last)
    lane = jnp.arange(chunk)[None, None, :]
    extra = jnp.where(
        lane == 0, parts[0], jnp.where(lane == 1, parts[1], jnp.where(lane == 2, parts[2], 0.0))
    ).astype(BF16)
    send_grad = (dot(picker, out_grad) * slot_weight).astype(BF16).reshape(sp_count, padded, -1)
    spot = jnp.arange(padded)[None, :, None]
    send_grad = jnp.where(spot == padded - 1, extra, send_grad)

    got_grad = lax.all_to_all(send_grad, "sp", 0, 0, tiled=True)
    got_rows = lax.all_to_all(send_rows, "sp", 0, 0, tiled=True)
    rows_own = got_rows[:, :capacity].reshape(slot_count, -1)
    grad_part = got_grad[:, :capacity].reshape(slot_count, -1)
    ends = jnp.sum(got_grad[:, capacity, :3].astype(F32), axis=1)
    grad_own = lax.all_gather(grad_part, "y", axis=1, tiled=True)
    rows_other = lax.ppermute(rows_own, "c", SWAP)
    grad_other = lax.ppermute(grad_own, "c", SWAP)

    gate_own, gate_other = (parity_rows(w_gate[0], k) for k in (core, 1 - core))
    up_own, up_other = (parity_rows(w_up[0], k) for k in (core, 1 - core))
    down_own, down_other = (parity_columns(w_down[0], k) for k in (core, 1 - core))
    gate = dot(rows_own, gate_own) + dot(rows_other, gate_other)
    up = dot(rows_own, up_own) + dot(rows_other, up_other)
    sig = jax.nn.sigmoid(gate)
    swish = gate * sig
    act = (swish * up).astype(BF16)
    act_grad = dot(grad_own, down_own, ACROSS) + dot(grad_other, down_other, ACROSS)
    gate_grad = (act_grad * up * sig * (1.0 + gate * (1.0 - sig))).astype(BF16)
    up_grad = (act_grad * swish).astype(BF16)

    partial_other = (
        dot(gate_grad, gate_other, ACROSS) + dot(up_grad, up_other, ACROSS)
    ).astype(BF16)
    arrived = lax.ppermute(partial_other, "c", SWAP)
    partial_own = dot(gate_grad, gate_own, ACROSS) + dot(up_grad, up_own, ACROSS)
    pair = (partial_own + arrived.astype(F32)).astype(BF16)
    pieces = jnp.moveaxis(pair.reshape(slot_count, 8, chunk), 1, 0)
    pieces = lax.all_to_all(pieces, "y", 0, 0, tiled=True)
    share = jnp.sum(pieces.astype(F32), axis=0).astype(BF16)

    gate_w_grad = joined_rows(
        dot(rows_own, gate_grad, ALONG).astype(BF16),
        dot(rows_other, gate_grad, ALONG).astype(BF16),
        core,
    )
    up_w_grad = joined_rows(
        dot(rows_own, up_grad, ALONG).astype(BF16),
        dot(rows_other, up_grad, ALONG).astype(BF16),
        core,
    )
    down_grad = joined_columns(
        dot(act, grad_own, ALONG).astype(BF16), dot(act, grad_other, ALONG).astype(BF16), core
    )

    returned = lax.all_to_all(
        share.reshape(sp_count, capacity, chunk), "sp", 0, 0, tiled=True
    )
    returned = jnp.pad(returned, ((0, 0), (0, padded - capacity), (0, 0)))
    token_grad = dot(picker, returned.reshape(sp_count * padded, chunk), ALONG)
    stream_part = (out_grad.astype(F32) + token_grad).astype(BF16)
    stream = lax.all_gather(stream_part, TP, axis=1, tiled=True)
    ret_grad = dot(stream, out_proj, ACROSS).astype(BF16)

    q, k, v, o = (a.astype(F32) for a in (queries, keys, values, ret_grad))
    rising = jnp.exp(running)[:, None]
    inject = dot(q * rising, o, ALONG)
    value_dim = values.shape[1]
    sent = jnp.broadcast_to(inject.astype(BF16)[None], (sp_count, *inject.shape))
    states = lax.all_to_all(sent, "sp", 0, 0, tiled=True)
    proj_part = dot(stream, retained, ALONG).astype(BF16)
    proj_parts = lax.all_to_all(
        proj_part.reshape(sp_count, width // sp_count, value_dim), "sp", 0, 0, tiled=True
    )
    out_proj_grad = jnp.sum(proj_parts.astype(F32), axis=0)

    order = jnp.arange(sp_count)
    between = (order[None, :] > block) & (order[None, :] < order[:, None])
    factors = jnp.where(
        order > block, jnp.exp(jnp.sum(jnp.where(between, ends[None, :], 0.0), axis=1)), 0.0
    )
    state_grad = jnp.sum(factors[:, None, None] * states.astype(F32), axis=0)

    place = jnp.arange(tokens)
    causal = place[:, None] >= place[None, :]
    diff = running[:, None] - running[None, :]
    decay = jnp.where(causal, jnp.exp(jnp.minimum(diff, 0.0)), 0.0)
    scores = dot(q, k, ACROSS) * decay
    prob_grad = dot(o, v, ACROSS) * decay
    tail = jnp.exp(last - running)[:, None]
    query_grad = dot(prob_grad, k) + rising * dot(o, incoming_state[0, 0], ACROSS)
    key_grad = dot(prob_grad, q, ALONG) + tail * dot(v, state_grad, ACROSS)
    value_grad = dot(scores, o, ALONG) + tail * dot(k, state_grad)
    return (
        gate_w_grad[None],
        up_w_grad[None],
        down_grad[None],
        out_proj_grad,
        query_grad.astype(BF16),
        key_grad.astype(BF16),
        value_grad.astype(BF16),
    )


def solution(mesh):
    torus = Mesh(mesh.devices.reshape(mesh.shape["sp"], 8, 2), ("sp", "y", "c"))
    placed = (
        P("sp", None),
        P("sp", TP),
        P("sp", None),
        P("sp", None),
        P("sp", None, TP),
        P("sp", None, TP),
        P("sp", TP, None),
        P(TP, None),
        P("sp", TP),
        P("sp", TP),
        P("sp", TP),
        P("sp", TP),
        P("sp", TP),
        P("sp", TP, None, None),
    )
    return jax.shard_map(
        on_device,
        mesh=torus,
        in_specs=placed,
        out_specs=(
            P("sp", None, TP),
            P("sp", None, TP),
            P("sp", TP, None),
            P("sp", TP),
            P("sp", TP),
            P("sp", TP),
            P("sp", TP),
        ),
        check_vma=False,
    )
```

time: 255 us -> 206 us (0.81)
  waiting for transfers between devices: 122 us -> 54.2 us
  starting transfers between devices: 26.2 us -> 51.5 us
  between operations: 15.2 us -> 2.54 us
  local copies, waits for them, and re-layouts: 9.55 us -> 20 us
  blocking collectives: 52.5 us -> 47.6 us
    all_gather x1 -> x0, waiting for transfers between devices: 47.4 us -> none  [sent_together_2(): whole, at, outs = (lax.all_gather(both, axis, axis=dim, tiled=True), 0, [])]
    all_to_all x1 -> x0, blocking collectives: 24.4 us -> none  [sent_together(): lax.all_to_all(both, axis, split_axis=split_dim, concat_axis=concat_dim,...]
    all_to_all x4 -> x6, waiting for transfers between devices: 74.4 us -> 54.2 us  [the longest x1 16.8 us: on_device(): pieces = lax.all_to_all(pieces, 'y', 0, 0, tiled=True)]
    all_gather x2, blocking collectives: 28.1 us -> 47.6 us  [the longest x1 28.6 us: on_device(): grad_own = lax.all_gather(grad_part, 'y', axis=1, tiled=True)]
    all_to_all x4 -> x6, starting transfers between devices: 26.1 us -> 45.1 us  [the longest x1 13.4 us: on_device(): got_grad = lax.all_to_all(send_grad, 'sp', 0, 0, tiled=True)]
    ppermute x0 -> x3, starting transfers between devices: none -> 6.36 us  [the longest x1 2.54 us: on_device(): rows_other = lax.ppermute(rows_own, 'c', SWAP)]
    dynamic_slice x0 -> x3, local copies, waits for them, and re-layouts: none -> 5.35 us  [the longest x2 3.19 us: parity_columns(): lax.dynamic_index_in_dim(x.reshape(rows, 8, 2, cols // 16), index, 2, kee...]
    concatenate x0 -> x3, local copies, waits for them, and re-layouts: none -> 3.26 us  [the longest x2 1.66 us: joined_rows(): return jnp.concatenate([first, second], axis=1).reshape(2 * rows, cols)]
  transfers between devices with their start and end apart: 5 -> 9, of which waited for: 5 -> 5; matrix products, arithmetic and copies ran while one was open for 5% -> 15% of each run, Pallas kernels for 0% -> 0%
where the time goes in v1:
time: 206 us; the launch traced here: 205 us
  waiting for transfers between devices  54.2 us (26%)
  starting transfers between devices  51.5 us (25%)
  blocking collectives  47.6 us (23%)
  matrix products  22.5 us (11%)
  local copies, waits for them, and re-layouts  20 us (10%)
  other arithmetic  6.51 us (3%)
  between operations  2.54 us (1%)
    all_gather x1, blocking collectives, on_device(): grad_own = lax.all_gather(grad_part, 'y', axis=1, tiled=True)  28.6 us
    dot_general x30, matrix products, dot(): return lax.dot_general(a, b, dims, preferred_element_type=F32)  22.5 us
    all_gather x1, blocking collectives, on_device(): stream = lax.all_gather(stream_part, TP, axis=1, tiled=True)  19.1 us
    all_to_all x1, waiting for transfers between devices, on_device(): pieces = lax.all_to_all(pieces, 'y', 0, 0, tiled=True)  16.8 us
    all_to_all x1, waiting for transfers between devices, on_device(): lax.all_to_all(proj_part.reshape(sp_count, width // sp_count, value_dim),...  13.7 us
    all_to_all x1, starting transfers between devices, on_device(): got_grad = lax.all_to_all(send_grad, 'sp', 0, 0, tiled=True)  13.4 us
    all_to_all x1, waiting for transfers between devices, on_device(): states = lax.all_to_all(sent, 'sp', 0, 0, tiled=True)  12.9 us
    all_to_all x1, starting transfers between devices, on_device(): lax.all_to_all(share.reshape(sp_count, capacity, chunk), 'sp', 0, 0, tile...  9.78 us
  transfers between devices with their start and end apart: 9, of which 5 were waited for; matrix products, arithmetic and copies ran while one was open for 15% of the time, Pallas kernels for 0%

profile of v1, /device:TPU:4, one launch (start us, length us, event | category | flops | bytes accessed | tf_op | source)
XLA Modules:
  0.0 204.8 jit_solution(3928460115457227741)
XLA Ops:
  6.6 1.2 fusion.1
  8.6 13.4 %all-to-all-start.1 = ((bf16[32,16,128]{2,1,0:T(8,128)(2,1)}), bf16[32,16,128]{2,1,0:T(8,128)(2,1)S(1)}, u32[]{:S(2)}, u32[]{:S(2)}) async-start(bf16[32,16,128]{2,1,0:T(8,128)(2,1)} %broadcast_select_fusion.4), calls=%async_computation.1 | async-start | bytes 262144 | tf_op jit(solution)/shard_map/all_to_all | solution.py:119
  22.6 2.3 %dynamic-slice_reduce_fusion = bf16[192,8,128]{2,1,0:T(8,128)(2,1)S(1)} fusion(bf16[192,8,2,128]{3,2,1,0:T(2,128)(2,1)S(1)} %reshape.287, s32[]{:T(128)S(6)} %select_n.175), kind=kLoop, calls=%fused_computation.37 | loop fusion | bytes 786436 | tf_op jit(solution)/shard_map/jit(dynamic_index_in_dim)/dynamic_slice | solution.py:42
  24.9 1.6 convolution_convert_fusion.1
  26.5 3.9 %all-to-all-done.1 = bf16[32,16,128]{2,1,0:T(8,128)(2,1)S(1)} async-done(((bf16[32,16,128]{2,1,0:T(8,128)(2,1)}), bf16[32,16,128]{2,1,0:T(8,128)(2,1)S(1)}, u32[]{:S(2)}, u32[]{:S(2)}) %all-to-all-start.1) | async-done | bytes 131104 | tf_op jit(solution)/shard_map/all_to_all | solution.py:119
  30.4 5.9 %all-to-all-start = ((bf16[32,16,1024]{2,1,0:T(8,128)(2,1)}), bf16[32,16,1024]{2,1,0:T(8,128)(2,1)S(1)}, u32[]{:S(2)}, u32[]{:S(2)}) async-start(bf16[32,16,1024]{2,1,0:T(8,128)(2,1)} %bitcast.7), calls=%async_computation | async-start | bytes 2097152 | tf_op jit(solution)/shard_map/all_to_all | solution.py:120
  36.4 28.6 %all_gather.6 = bf16[480,1024]{1,0:T(8,128)(2,1)S(1)} all-gather(bf16[480,128]{1,0:T(8,128)(2,1)S(1)} %reshape.294), channel_id=1, replica_groups=mesh['sp'=32,'y'=8,'c'=2] {'y'}, dimensions={1}, use_global_device_ids=true | all-gather | bytes 1105920 | tf_op jit(solution)/shard_map/all_gather | solution.py:124
  65.0 1.9 collective-permute-start
  66.9 1.3 copy.47
  69.0 2.2 %constant_dynamic-slice_fusion = (bf16[8,1,128,128]{3,2,1,0:T(8,128)(2,1)}, bf16[8,1,128,128]{3,2,1,0:T(8,128)(2,1)}, bf16[8,1,128,128]{3,2,1,0:T(8,128)(2,1)}, bf16[8,1,128,128]{3,2,1,0:T(8,128)(2,1)}) fusion(bf16[8,2,128,128]{3,2,1,0:T(8,128)(2,1)} %bitcast.158, s32[]{:T(128)S(6)} %select_n.182, s32[]{:T(128)S(6)} %select_n.175, ...), kind=kLoop, calls=%fused_computation.88 | loop fusion | bytes 2097160 | tf_op jit(solution)/shard_map/jit(dynamic_index_in_dim)/dynamic_slice | solution.py:49
  71.5 2.5 %collective-permute-start.1 = (bf16[480,1024]{1,0:T(8,128)(2,1)S(1)}, bf16[480,1024]{1,0:T(8,128)(2,1)S(1)}, u32[]{:S(2)}, u32[]{:S(2)}) collective-permute-start(bf16[480,1024]{1,0:T(8,128)(2,1)S(1)} %reshape.290), channel_id=1, source_target_pairs={{0,1},{1,0},{2,3},{3,2},{4,5},{5,4},{6,7},{7,6},{8,9},{9,8},{10,11... | collective-permute-start | bytes 2949128 | tf_op jit(solution)/shard_map/ppermute | solution.py:125
  74.1 1.4 fusion.43
  75.5 1.7 convolution_add_fusion.2
  80.1 1.4 add_convert_fusion.1
  81.5 1.9 collective-permute-start.2
  84.2 1.2 fusion.27
  85.5 1.4 fusion.46
  86.9 1.6 fusion
  89.6 4.4 %all-to-all-start.2 = ((bf16[8,480,128]{2,1,0:T(8,128)(2,1)}), bf16[8,480,128]{2,1,0:T(8,128)(2,1)}, u32[]{:S(2)}, u32[]{:S(2)}) async-start(bf16[8,480,128]{2,1,0:T(8,128)(2,1)} %bitcast.137), calls=%async_computation.2 | async-start | bytes 1966080 | tf_op jit(solution)/shard_map/all_to_all | solution.py:147
  94.1 1.2 convolution_convert_fusion.3
  95.3 1.6 select_bitcast_fusion.1
  97.1 1.6 copy.50
  98.7 2.2 %broadcast_in_dim_reshape.11 = bf16[1,128,2048]{2,1,0:T(8,128)(2,1)} reshape(bf16[128,8,2,128]{3,2,1,0:T(2,128)(2,1)} %copy.50) | data formatting | bytes 1048576 | tf_op jit(solution)/shard_map/broadcast_in_dim;reshape | solution.py:205
  102.9 16.8 %all-to-all-done.2 = bf16[8,480,128]{2,1,0:T(8,128)(2,1)} async-done(((bf16[8,480,128]{2,1,0:T(8,128)(2,1)}), bf16[8,480,128]{2,1,0:T(8,128)(2,1)}, u32[]{:S(2)}, u32[]{:S(2)}) %all-to-all-start.2) | async-done | bytes 983072 | tf_op jit(solution)/shard_map/all_to_all | solution.py:147
  119.8 1.3 reduce_sum.88
  121.8 9.8 %all-to-all-start.3 = ((bf16[32,15,128]{2,1,0:T(8,128)(2,1)}), bf16[32,15,128]{2,1,0:T(8,128)(2,1)S(1)}, u32[]{:S(2)}, u32[]{:S(2)}) async-start(bf16[32,15,128]{2,1,0:T(8,128)(2,1)} %reshape.302), calls=%async_computation.3 | async-start | bytes 262144 | tf_op jit(solution)/shard_map/all_to_all | solution.py:164
  133.4 6.8 %all-to-all-done.3 = bf16[32,15,128]{2,1,0:T(8,128)(2,1)S(1)} async-done(((bf16[32,15,128]{2,1,0:T(8,128)(2,1)}), bf16[32,15,128]{2,1,0:T(8,128)(2,1)S(1)}, u32[]{:S(2)}, u32[]{:S(2)}) %all-to-all-start.3) | async-done | bytes 122912 | tf_op jit(solution)/shard_map/all_to_all | solution.py:164
  140.6 19.1 %all_gather.7 = bf16[192,2048]{1,0:T(8,128)(2,1)S(1)} all-gather(bf16[192,128]{1,0:T(8,128)(2,1)S(1)} %fusion.6), channel_id=1, replica_groups=mesh['sp'=32,'y'=8,'c'=2] {'y','c'}, dimensions={1}, use_global_device_ids=true | all-gather | bytes 835584 | tf_op jit(solution)/shard_map/all_gather | solution.py:170
  161.3 6.0 %all-to-all-start.5 = ((bf16[32,48,96]{2,1,0:T(8,128)(2,1)}), bf16[32,48,96]{2,1,0:T(8,128)(2,1)S(1)}, u32[]{:S(2)}, u32[]{:S(2)}) async-start(bf16[32,48,96]{2,1,0:T(8,128)(2,1)} %broadcast_in_dim.121), calls=%async_computation.5 | async-start | bytes 786432 | tf_op jit(solution)/shard_map/all_to_all | solution.py:178
  169.3 12.9 %all-to-all-done.5 = bf16[32,48,96]{2,1,0:T(8,128)(2,1)S(1)} async-done(((bf16[32,48,96]{2,1,0:T(8,128)(2,1)}), bf16[32,48,96]{2,1,0:T(8,128)(2,1)S(1)}, u32[]{:S(2)}, u32[]{:S(2)}) %all-to-all-start.5) | async-done | bytes 294944 | tf_op jit(solution)/shard_map/all_to_all | solution.py:178
  182.2 5.6 %all-to-all-start.4 = ((bf16[32,64,96]{2,1,0:T(8,128)(2,1)}), bf16[32,64,96]{2,1,0:T(8,128)(2,1)S(1)}, u32[]{:S(2)}, u32[]{:S(2)}) async-start(bf16[32,64,96]{2,1,0:T(8,128)(2,1)} %bitcast.33), calls=%async_computation.4 | async-start | bytes 1048576 | tf_op jit(solution)/shard_map/all_to_all | solution.py:180
  190.4 13.7 %all-to-all-done.4 = bf16[32,64,96]{2,1,0:T(8,128)(2,1)S(1)} async-done(((bf16[32,64,96]{2,1,0:T(8,128)(2,1)}), bf16[32,64,96]{2,1,0:T(8,128)(2,1)S(1)}, u32[]{:S(2)}, u32[]{:S(2)}) %all-to-all-start.4) | async-done | bytes 393248 | tf_op jit(solution)/shard_map/all_to_all | solution.py:180
  (98 shorter events, 23.8 us)
Async XLA Ops:
  0.6 159.0 %copy-start = (bf16[96,2048]{1,0:T(8,128)(2,1)S(1)}, bf16[96,2048]{1,0:T(8,128)(2,1)}, u32[]{:S(2)}) copy-start(bf16[96,2048]{1,0:T(8,128)(2,1)} %param.21) | copy-start | bytes 1179652
  0.6 21.4 %copy-start.9 = (bf16[192,2048]{1,0:T(8,128)(2,1)S(1)}, bf16[192,2048]{1,0:T(8,128)(2,1)}, u32[]{:S(2)}) copy-start(bf16[192,2048]{1,0:T(8,128)(2,1)} %param.14) | copy-start | bytes 2359300
  8.6 21.9 %all-to-all-start.1 = ((bf16[32,16,128]{2,1,0:T(8,128)(2,1)}), bf16[32,16,128]{2,1,0:T(8,128)(2,1)S(1)}, u32[]{:S(2)}, u32[]{:S(2)}) async-start(bf16[32,16,128]{2,1,0:T(8,128)(2,1)} %broadcast_select_fusion.4), calls=%async_computation.1 | async-start | bytes 262144 | tf_op jit(solution)/shard_map/all_to_all | solution.py:119
  30.4 5.9 %copy-start.10 = (bf16[32,16,128]{2,1,0:T(8,128)(2,1)}, bf16[32,16,128]{2,1,0:T(8,128)(2,1)S(1)}, u32[]{:S(2)}) copy-start(bf16[32,16,128]{2,1,0:T(8,128)(2,1)S(1)} %all-to-all-done.1) | copy-start | bytes 393220
  30.4 40.8 %all-to-all-start = ((bf16[32,16,1024]{2,1,0:T(8,128)(2,1)}), bf16[32,16,1024]{2,1,0:T(8,128)(2,1)S(1)}, u32[]{:S(2)}, u32[]{:S(2)}) async-start(bf16[32,16,1024]{2,1,0:T(8,128)(2,1)} %bitcast.7), calls=%async_computation | async-start | bytes 2097152 | tf_op jit(solution)/shard_map/all_to_all | solution.py:120
  65.0 10.5 %collective-permute-start = (bf16[480,1024]{1,0:T(8,128)(2,1)S(1)}, bf16[480,1024]{1,0:T(8,128)(2,1)}, u32[]{:S(2)}, u32[]{:S(2)}) collective-permute-start(bf16[480,1024]{1,0:T(8,128)(2,1)S(1)} %all_gather.6), channel_id=1, source_target_pairs={{0,1},{1,0},{2,3},{3,2},{4,5},{5,4},{6,7},{7,6},{8,9},{9,8},{10,11... | collective-permute-start | bytes 2949128 | tf_op jit(solution)/shard_map/ppermute | solution.py:126
  71.5 5.7 %copy-start.3 = (bf16[8,1,128,128]{3,2,1,0:T(8,128)(2,1)S(1)}, bf16[8,1,128,128]{3,2,1,0:T(8,128)(2,1)}, u32[]{:S(2)}) copy-start(bf16[8,1,128,128]{3,2,1,0:T(8,128)(2,1)} %get-tuple-element.20) | copy-start | bytes 786436
  71.5 6.6 %collective-permute-start.1 = (bf16[480,1024]{1,0:T(8,128)(2,1)S(1)}, bf16[480,1024]{1,0:T(8,128)(2,1)S(1)}, u32[]{:S(2)}, u32[]{:S(2)}) collective-permute-start(bf16[480,1024]{1,0:T(8,128)(2,1)S(1)} %reshape.290), channel_id=1, source_target_pairs={{0,1},{1,0},{2,3},{3,2},{4,5},{5,4},{6,7},{7,6},{8,9},{9,8},{10,11... | collective-permute-start | bytes 2949128 | tf_op jit(solution)/shard_map/ppermute | solution.py:125
  75.5 2.2 %copy-start.1 = (bf16[8,1,128,128]{3,2,1,0:T(8,128)(2,1)S(1)}, bf16[8,1,128,128]{3,2,1,0:T(8,128)(2,1)}, u32[]{:S(2)}) copy-start(bf16[8,1,128,128]{3,2,1,0:T(8,128)(2,1)} %get-tuple-element.33) | copy-start | bytes 786436
  75.5 2.6 %copy-start.4 = (bf16[8,1,128,128]{3,2,1,0:T(8,128)(2,1)S(1)}, bf16[8,1,128,128]{3,2,1,0:T(8,128)(2,1)}, u32[]{:S(2)}) copy-start(bf16[8,1,128,128]{3,2,1,0:T(8,128)(2,1)} %get-tuple-element.19) | copy-start | bytes 786436
  77.7 1.0 copy-start.8
  79.7 1.8 copy-start.5
  81.5 5.3 %collective-permute-start.2 = (bf16[480,1024]{1,0:T(8,128)(2,1)}, bf16[480,1024]{1,0:T(8,128)(2,1)}, u32[]{:S(2)}, u32[]{:S(2)}) collective-permute-start(bf16[480,1024]{1,0:T(8,128)(2,1)} %add_convert_fusion.1), channel_id=1, source_target_pairs={{0,1},{1,0},{2,3},{3,2},{4,5},{5,4},{6,7},{7,6},{8,9},{9,8},{10,11... | collective-permute-start | bytes 2949128 | tf_op jit(solution)/shard_map/ppermute | solution.py:143
  83.5 3.4 %copy-start.2 = (bf16[8,1,128,128]{3,2,1,0:T(8,128)(2,1)S(1)}, bf16[8,1,128,128]{3,2,1,0:T(8,128)(2,1)}, u32[]{:S(2)}) copy-start(bf16[8,1,128,128]{3,2,1,0:T(8,128)(2,1)} %get-tuple-element.33) | copy-start | bytes 786436
  83.5 3.4 %copy-start.6 = (bf16[480,128]{1,0:T(8,128)(2,1)S(1)}, bf16[480,128]{1,0:T(8,128)(2,1)}, u32[]{:S(2)}) copy-start(bf16[480,128]{1,0:T(8,128)(2,1)} %copy-done.5) | copy-start | bytes 368644
  89.6 30.1 %all-to-all-start.2 = ((bf16[8,480,128]{2,1,0:T(8,128)(2,1)}), bf16[8,480,128]{2,1,0:T(8,128)(2,1)}, u32[]{:S(2)}, u32[]{:S(2)}) async-start(bf16[8,480,128]{2,1,0:T(8,128)(2,1)} %bitcast.137), calls=%async_computation.2 | async-start | bytes 1966080 | tf_op jit(solution)/shard_map/all_to_all | solution.py:147
  97.1 4.3 %copy-start.7 = (bf16[480,128]{1,0:T(8,128)(2,1)S(1)}, bf16[480,128]{1,0:T(8,128)(2,1)}, u32[]{:S(2)}) copy-start(bf16[480,128]{1,0:T(8,128)(2,1)} %copy-done.5) | copy-start | bytes 368644
  121.8 18.4 %all-to-all-start.3 = ((bf16[32,15,128]{2,1,0:T(8,128)(2,1)}), bf16[32,15,128]{2,1,0:T(8,128)(2,1)S(1)}, u32[]{:S(2)}, u32[]{:S(2)}) async-start(bf16[32,15,128]{2,1,0:T(8,128)(2,1)} %reshape.302), calls=%async_computation.3 | async-start | bytes 262144 | tf_op jit(solution)/shard_map/all_to_all | solution.py:164
  131.7 8.6 %copy-start.16 = (bf16[192,128]{1,0:T(8,128)(2,1)S(1)}, bf16[192,128]{1,0:T(8,128)(2,1)}, u32[]{:S(2)}) copy-start(bf16[192,128]{1,0:T(8,128)(2,1)} %param.15) | copy-start | bytes 147460
  132.5 27.5 %copy-start.13 = (bf16[192,96]{1,0:T(8,128)(2,1)S(1)}, bf16[192,96]{1,0:T(8,128)(2,1)}, u32[]{:S(2)}) copy-start(bf16[192,96]{1,0:T(8,128)(2,1)} %param.22) | copy-start | bytes 110596
  140.3 20.1 %copy-start.11 = (bf16[192,48]{0,1:T(8,128)(2,1)S(1)}, bf16[192,48]{0,1:T(8,128)(2,1)}, u32[]{:S(2)}) copy-start(bf16[192,48]{0,1:T(8,128)(2,1)} %param.23) | copy-start | bytes 55300
  159.6 7.7 %copy-start.14 = (bf16[192,96]{1,0:T(8,128)(2,1)S(1)}, bf16[192,96]{1,0:T(8,128)(2,1)}, u32[]{:S(2)}) copy-start(bf16[192,96]{1,0:T(8,128)(2,1)} %param.25) | copy-start | bytes 110596
  160.0 8.7 %copy-start.12 = (bf16[192,48]{0,1:T(8,128)(2,1)S(1)}, bf16[192,48]{0,1:T(8,128)(2,1)}, u32[]{:S(2)}) copy-start(bf16[192,48]{0,1:T(8,128)(2,1)} %param.24) | copy-start | bytes 55300
  161.3 26.5 %copy-start.15 = (f32[1,1,48,96]{3,2,1,0:T(8,128)S(1)}, f32[1,1,48,96]{3,2,1,0:T(8,128)}, u32[]{:S(2)}) copy-start(f32[1,1,48,96]{3,2,1,0:T(8,128)} %param.27) | copy-start | bytes 55300
  161.3 20.9 %all-to-all-start.5 = ((bf16[32,48,96]{2,1,0:T(8,128)(2,1)}), bf16[32,48,96]{2,1,0:T(8,128)(2,1)S(1)}, u32[]{:S(2)}, u32[]{:S(2)}) async-start(bf16[32,48,96]{2,1,0:T(8,128)(2,1)} %broadcast_in_dim.121), calls=%async_computation.5 | async-start | bytes 786432 | tf_op jit(solution)/shard_map/all_to_all | solution.py:178
  182.2 21.9 %all-to-all-start.4 = ((bf16[32,64,96]{2,1,0:T(8,128)(2,1)}), bf16[32,64,96]{2,1,0:T(8,128)(2,1)S(1)}, u32[]{:S(2)}, u32[]{:S(2)}) async-start(bf16[32,64,96]{2,1,0:T(8,128)(2,1)} %bitcast.33), calls=%async_computation.4 | async-start | bytes 1048576 | tf_op jit(solution)/shard_map/all_to_all | solution.py:180

commit v2 on v1

v2 whole, which is shorter than its diff:
```python
import functools

import jax
import jax.numpy as jnp
from jax import lax
from jax.experimental import pallas as pl
from jax.experimental.pallas import tpu as pltpu
from jax.sharding import Mesh
from jax.sharding import PartitionSpec as P

TP = ("y", "c")
F32 = jnp.float32
BF16 = jnp.bfloat16
PLAIN = (((1,), (0,)), ((), ()))
ACROSS = (((1,), (1,)), ((), ()))
ALONG = (((0,), (0,)), ((), ()))
SWAP = [(0, 1), (1, 0)]
VMEM = pl.BlockSpec(memory_space=pltpu.VMEM)
SMEM = pl.BlockSpec(memory_space=pltpu.SMEM)


def dot(a, b, dims=PLAIN):
    return lax.dot_general(a, b, dims, preferred_element_type=F32)


def call(body, ins, outs, name, scratch=(), flops=0, limit=20):
    specs = [SMEM if k == "s" else VMEM for k, _ in ins]
    arrays = [a for _, a in ins]
    return pl.pallas_call(
        body,
        in_specs=specs,
        out_specs=tuple(VMEM for _ in outs),
        out_shape=tuple(jax.ShapeDtypeStruct(s, d) for s, d in outs),
        scratch_shapes=list(scratch),
        name=name,
        compiler_params=pltpu.CompilerParams(vmem_limit_bytes=limit << 20),
        cost_estimate=pl.CostEstimate(flops=flops, transcendentals=0, bytes_accessed=0),
    )(*arrays)


def in_three(x):
    high = x.astype(BF16)
    rest = x - high.astype(F32)
    middle = rest.astype(BF16)
    low = (rest - middle.astype(F32)).astype(BF16)
    return high, middle, low


def setup_body(ids_ref, weight_ref, grad_ref, picker_ref, send_ref, *, experts, padded):
    tokens = ids_ref.shape[1]
    slots = experts * padded
    grad = grad_ref[...].astype(F32)
    row = lax.broadcasted_iota(jnp.int32, (tokens, tokens), 0)
    col = lax.broadcasted_iota(jnp.int32, (tokens, tokens), 1)
    same = jnp.where(row == col, 1.0, 0.0).astype(BF16)
    earlier = jnp.where(row > col, 1.0, 0.0).astype(BF16)
    lines = jnp.concatenate(
        [ids_ref[...].astype(F32)] + [p.astype(F32) for p in in_three(weight_ref[...])], axis=0
    )
    columns = dot(same, lines.astype(BF16), ACROSS)
    ids = columns[:, :2]
    names = lax.broadcasted_iota(jnp.int32, (tokens, experts), 1).astype(F32)
    onehot = [jnp.where(ids[:, j : j + 1] == names, 1.0, 0.0) for j in (0, 1)]
    before = dot(earlier, (onehot[0] + onehot[1]).astype(BF16))
    spots = lax.broadcasted_iota(jnp.int32, (tokens, slots), 1)
    picker, sent = None, None
    for j in (0, 1):
        rank = jnp.sum(before * onehot[j], axis=1, keepdims=True)
        slot = (ids[:, j : j + 1] * padded + rank).astype(jnp.int32)
        hits = jnp.where(spots == slot, 1.0, 0.0).astype(BF16)
        high, middle, low = (columns[:, k + j : k + j + 1] for k in (2, 4, 6))
        weight = (high + middle) + low
        part = dot(hits, (grad * weight).astype(BF16), ALONG)
        picker = hits if picker is None else picker + hits
        sent = part if sent is None else sent + part
    picker_ref[...] = picker
    send_ref[...] = sent.astype(BF16)


def rows_body(core_ref, picker_ref, input_ref, decay_ref, send_ref, *, padded):
    rows = dot(picker_ref[...], half_columns(input_ref, core_ref[0]), ALONG)
    parts = in_three(jnp.sum(decay_ref[...], axis=1, keepdims=True))
    lane = lax.broadcasted_iota(jnp.int32, rows.shape, 1)
    row = lax.broadcasted_iota(jnp.int32, rows.shape, 0)
    extra = jnp.zeros((1, 1), F32)
    for k, part in enumerate(parts):
        extra = jnp.where(lane == k, part.astype(F32), extra)
    send_ref[...] = jnp.where((row & (padded - 1)) == padded - 1, extra, rows).astype(BF16)


def half_weights(ref, core):
    chunks = ref[:, core]
    return chunks.reshape(chunks.shape[0] * chunks.shape[1], chunks.shape[2])


def half_columns(ref, core):
    chunk = 128
    pieces = [
        ref[:, pl.ds(pl.multiple_of((2 * k + core) * chunk, chunk), chunk)]
        for k in range(ref.shape[1] // (2 * chunk))
    ]
    return jnp.concatenate(pieces, axis=1)


def own_body(core_ref, rows_ref, grad_ref, gate_ref, up_ref, down_ref, hidden_ref, back_ref):
    core = core_ref[0]
    both = jnp.concatenate([half_weights(gate_ref, core), half_weights(up_ref, core)], axis=1)
    hidden_ref[...] = dot(rows_ref[...], both)
    back_ref[...] = dot(grad_ref[...], half_columns(down_ref, core), ACROSS)


def other_body(
    core_ref, rows_ref, grad_ref, gate_ref, up_ref, down_ref, hidden_ref, back_ref,
    act_ref, both_ref, full_ref,
):
    core = 1 - core_ref[0]
    short = grad_ref.shape[0]
    both = jnp.concatenate([half_weights(gate_ref, core), half_weights(up_ref, core)], axis=1)
    hidden = hidden_ref[...] + dot(rows_ref[...], both)
    full_ref[pl.ds(full_ref.shape[0] - 8, 8), :] = jnp.zeros((8, full_ref.shape[1]), F32)
    full_ref[pl.ds(0, short), :] = back_ref[...] + dot(
        grad_ref[...], half_columns(down_ref, core), ACROSS
    )
    act_grad = full_ref[...]
    units = act_grad.shape[1]
    gate, up = hidden[:, :units], hidden[:, units:]
    sig = jax.nn.sigmoid(gate)
    swish = gate * sig
    act_ref[...] = (swish * up).astype(BF16)[:short]
    both_ref[:, :units] = (act_grad * up * sig * (1.0 + gate * (1.0 - sig))).astype(BF16)
    both_ref[:, units:] = (act_grad * swish).astype(BF16)


def input_grad_body(core_ref, mine_ref, pair_ref, gate_ref, up_ref, cross_ref, out_ref):
    core = core_ref[0]
    grads = jnp.concatenate([mine_ref[...], pair_ref[...]], axis=1)
    gate, up, cross = gate_ref[:, core], up_ref[:, core], cross_ref[...]
    weights = jnp.concatenate([gate, up, cross], axis=2)
    for k in range(0, weights.shape[0], 2):
        two = weights[k : k + 2].reshape(2 * weights.shape[1], weights.shape[2])
        found = dot(grads, two, ACROSS).astype(BF16)
        out_ref[k] = found[:, : weights.shape[1]]
        out_ref[k + 1] = found[:, weights.shape[1] :]


def sum_body(parts_ref, out_ref):
    total = parts_ref[0].astype(F32)
    for k in range(1, parts_ref.shape[0]):
        total = total + parts_ref[k].astype(F32)
    out_ref[...] = total.astype(BF16)


def pack_body(stream_ref, proj_ref, kept_ref, query_ref, rising_ref, ret_ref, pay_ref):
    stream = stream_ref[...]
    ret = dot(stream, proj_ref[...], ACROSS).astype(BF16)
    ret_ref[...] = ret
    inject = dot((query_ref[...].astype(F32) * rising_ref[...]).astype(BF16), ret, ALONG)
    proj = dot(stream, kept_ref[...], ALONG)
    count, rows, lanes = pay_ref.shape
    each = proj.shape[0] // count
    width = proj.shape[1]
    whole = rows - inject.shape[0]
    rest = each - whole
    fold = lanes - width
    blank = jnp.zeros((rows - rest * (width // fold), fold), F32)
    for m in range(count):
        own = proj[m * each : (m + 1) * each]
        left = jnp.concatenate([inject, own[:whole]], axis=0)
        right = jnp.concatenate(
            [own[whole:, k * fold : (k + 1) * fold] for k in range(width // fold)] + [blank],
            axis=0,
        )
        pay_ref[m] = jnp.concatenate([left, right], axis=1).astype(BF16)


def last_body(
    factor_ref, got_ref, keys_ref, values_ref, tail_ref, tail_row_ref, key_part_ref,
    value_part_ref, key_ref, value_ref, proj_ref,
):
    count, rows, lanes = got_ref.shape
    key_dim, width = keys_ref.shape[1], values_ref.shape[1]
    state, total = None, None
    for m in range(count):
        part = got_ref[m].astype(F32)
        total = part if total is None else total + part
        scaled = factor_ref[m] * part[:key_dim]
        state = scaled if state is None else state + scaled
    state = state[:, :width].astype(BF16)
    fold = lanes - width
    whole = rows - key_dim
    rest = proj_ref.shape[0] - whole
    proj_ref[:whole, :] = total[key_dim:, :width]
    proj_ref[whole:, :] = jnp.concatenate(
        [total[k * rest : (k + 1) * rest, width:] for k in range(width // fold)], axis=1
    )
    tail = tail_ref[...]
    across = dot(state, values_ref[...], ACROSS)
    key_ref[...] = (key_part_ref[...] + tail_row_ref[...] * across).astype(BF16)
    value_ref[...] = (value_part_ref[...] + tail * dot(keys_ref[...], state)).astype(BF16)


def parity_columns(x, index):
    rows, cols = x.shape
    return lax.dynamic_index_in_dim(
        x.reshape(rows, 8, 2, cols // 16), index, 2, keepdims=False
    ).reshape(rows, cols // 2)


def joined_rows(own, other, core):
    rows, cols = own.shape
    own, other = (a.reshape(8, 1, rows // 8, cols) for a in (own, other))
    first = jnp.where(core == 0, own, other)
    second = jnp.where(core == 0, other, own)
    return jnp.concatenate([first, second], axis=1).reshape(2 * rows, cols)


def joined_columns(own, other, core):
    rows, cols = own.shape
    own, other = (a.reshape(rows, 8, 1, cols // 8) for a in (own, other))
    first = jnp.where(core == 0, own, other)
    second = jnp.where(core == 0, other, own)
    return jnp.concatenate([first, second], axis=2).reshape(rows, 2 * cols)


def on_device(
    moe_input,
    out_grad,
    expert_ids,
    expert_weights,
    w_gate,
    w_up,
    w_down,
    out_proj,
    retained,
    queries,
    keys,
    values,
    log_decay,
    incoming_state,
):
    tokens, width = moe_input.shape
    sp_count = lax.axis_size("sp")
    padded = 16
    slots = sp_count * padded
    short = slots - 1
    core = lax.axis_index("c")
    block = lax.axis_index("sp")
    chunk = out_grad.shape[1]
    half = width // 2
    units = w_gate.shape[2]
    key_dim, value_dim = queries.shape[1], values.shape[1]

    core_1 = core.astype(jnp.int32).reshape(1)
    picker, send_grad = call(
        functools.partial(setup_body, experts=sp_count, padded=padded),
        [("v", expert_ids.T), ("v", expert_weights.T), ("v", out_grad)],
        [((tokens, slots), BF16), ((slots, chunk), BF16)],
        "setup",
    )
    with jax.named_scope("grad_send"):
        got_grad = lax.all_to_all(
            send_grad.reshape(sp_count, padded, chunk), "sp", 0, 0, tiled=True
        )
    got_grad = got_grad.reshape(slots, chunk)[:short]

    (send_rows,) = call(
        functools.partial(rows_body, padded=padded),
        [("s", core_1), ("v", picker), ("v", moe_input), ("v", log_decay.T)],
        [((slots, half), BF16)],
        "rows",
    )
    gate_4 = w_gate.reshape(8, 2, chunk, units)
    up_4 = w_up.reshape(8, 2, chunk, units)
    down_2 = w_down[0]
    cross_sent = jnp.concatenate(
        [lax.dynamic_index_in_dim(w, 1 - core, 1, keepdims=False) for w in (gate_4, up_4)], axis=2
    )
    with jax.named_scope("cross_send"):
        cross = lax.ppermute(cross_sent, "c", SWAP)

    send_rows, got_grad, cross = lax.optimization_barrier((send_rows, got_grad, cross))
    send_rows = send_rows.reshape(sp_count, padded, half)
    with jax.named_scope("rows_send"):
        got_rows = lax.all_to_all(send_rows, "sp", 0, 0, tiled=True)
    ends = jnp.sum(got_rows[:, padded - 1, :3].astype(F32), axis=1)
    rows_own = got_rows.reshape(slots, half)
    running = jnp.cumsum(log_decay[:, 0])
    last = running[-1]

    with jax.named_scope("grad_gather"):
        grad_own = lax.all_gather(got_grad, "y", axis=1, tiled=True)
    rows_own, grad_own = lax.optimization_barrier((rows_own, grad_own))
    rows_other = lax.ppermute(rows_own, "c", SWAP)
    grad_other = lax.ppermute(grad_own, "c", SWAP)

    hidden, back = call(
        own_body,
        [("s", core_1), ("v", rows_own), ("v", grad_own), ("v", gate_4), ("v", up_4), ("v", down_2)],
        [((slots, 2 * units), F32), ((short, units), F32)],
        "own_half",
        flops=6 * slots * half * units,
    )
    act, both = call(
        other_body,
        [
            ("s", core_1), ("v", rows_other), ("v", grad_other), ("v", gate_4), ("v", up_4),
            ("v", down_2), ("v", hidden), ("v", back),
        ],
        [((short, units), BF16), ((slots, 2 * units), BF16)],
        "other_half",
        scratch=[pltpu.VMEM((slots, units), F32)],
        flops=6 * slots * half * units,
    )
    pair_both = lax.ppermute(both, "c", SWAP)
    (pieces,) = call(
        input_grad_body,
        [
            ("s", core_1), ("v", both), ("v", pair_both), ("v", gate_4), ("v", up_4), ("v", cross),
        ],
        [((8, slots, chunk), BF16)],
        "input_grad",
        flops=8 * slots * half * units,
    )
    pieces = lax.all_to_all(pieces, "y", 0, 0, tiled=True)

    w_own, w_other = (dot(r, both, ALONG).astype(BF16) for r in (rows_own, rows_other))
    w_grads = joined_rows(w_own, w_other, core)
    gate_w_grad, up_w_grad = w_grads[:, :units], w_grads[:, units:]
    down_grad = joined_columns(
        dot(act, grad_own, ALONG).astype(BF16), dot(act, grad_other, ALONG).astype(BF16), core
    )

    (share,) = call(sum_body, [("v", pieces)], [((slots, chunk), BF16)], "add_parts")
    returned = lax.all_to_all(
        share.reshape(sp_count, padded, chunk), "sp", 0, 0, tiled=True
    ).reshape(slots, chunk)
    stream_part = (out_grad.astype(F32) + dot(picker, returned)).astype(BF16)
    stream = lax.all_gather(stream_part, TP, axis=1, tiled=True)

    rising = jnp.exp(running)[:, None]
    whole = 40
    ret_grad, payload = call(
        pack_body,
        [("v", stream), ("v", out_proj), ("v", retained), ("v", queries), ("v", rising)],
        [((tokens, value_dim), BF16), ((sp_count, key_dim + whole, 128), BF16)],
        "pack",
        flops=4 * tokens * width * value_dim,
    )
    got = lax.all_to_all(payload, "sp", 0, 0, tiled=True)

    order = jnp.arange(sp_count)
    between = (order[None, :] > block) & (order[None, :] < order[:, None])
    factors = jnp.where(
        order > block, jnp.exp(jnp.sum(jnp.where(between, ends[None, :], 0.0), axis=1)), 0.0
    )
    q, k, v, o = (a.astype(F32) for a in (queries, keys, values, ret_grad))
    place = jnp.arange(tokens)
    causal = place[:, None] >= place[None, :]
    diff = running[:, None] - running[None, :]
    decay = jnp.where(causal, jnp.exp(jnp.minimum(diff, 0.0)), 0.0)
    scores = dot(q, k, ACROSS) * decay
    prob_grad = dot(o, v, ACROSS) * decay
    tail = jnp.exp(last - running)[:, None]
    query_grad = dot(prob_grad, k) + rising * dot(o, incoming_state[0, 0], ACROSS)
    key_part = dot(q, prob_grad, ALONG)
    value_part = dot(scores, o, ALONG)
    key_grad, value_grad, out_proj_grad = call(
        last_body,
        [
            ("s", factors), ("v", got), ("v", keys), ("v", values), ("v", tail),
            ("v", tail.T), ("v", key_part), ("v", value_part),
        ],
        [
            ((key_dim, tokens), BF16), ((tokens, value_dim), BF16),
            ((width // sp_count, value_dim), F32),
        ],
        "finish",
    )
    return (
        gate_w_grad[None],
        up_w_grad[None],
        down_grad[None],
        out_proj_grad,
        query_grad.astype(BF16),
        key_grad.T,
        value_grad,
    )


def solution(mesh):
    torus = Mesh(mesh.devices.reshape(mesh.shape["sp"], 8, 2), ("sp", "y", "c"))
    placed = (
        P("sp", None),
        P("sp", TP),
        P("sp", None),
        P("sp", None),
        P("sp", None, TP),
        P("sp", None, TP),
        P("sp", TP, None),
        P(TP, None),
        P("sp", TP),
        P("sp", TP),
        P("sp", TP),
        P("sp", TP),
        P("sp", TP),
        P("sp", TP, None, None),
    )
    return jax.shard_map(
        on_device,
        mesh=torus,
        in_specs=placed,
        out_specs=(
            P("sp", None, TP),
            P("sp", None, TP),
            P("sp", TP, None),
            P("sp", TP),
            P("sp", TP),
            P("sp", TP),
            P("sp", TP),
        ),
        check_vma=False,
    )
```

time: 206 us -> 184 us (0.89)
  the two profiles are of different devices: /device:TPU:4 before, /device:TPU:8 now
where the time goes in v2:
time: 184 us; the launch traced here: 182 us
  waiting for transfers between devices  51.8 us (28%)
  blocking collectives  47.1 us (26%)
  starting transfers between devices  44.2 us (24%)
  local copies, waits for them, and re-layouts  16.6 us (9%)
  Pallas kernels  12.9 us (7%)
  matrix products  6.46 us (4%)
  other arithmetic  2.29 us (1%)
    all_gather x1, blocking collectives, on_device(): grad_own = lax.all_gather(got_grad, 'y', axis=1, tiled=True)  29 us
    all_gather x1, blocking collectives, on_device(): stream = lax.all_gather(stream_part, TP, axis=1, tiled=True)  18.1 us
    all_to_all x1, waiting for transfers between devices, on_device(): got = lax.all_to_all(payload, 'sp', 0, 0, tiled=True)  17.6 us
    all_to_all x1, waiting for transfers between devices, on_device(): pieces = lax.all_to_all(pieces, 'y', 0, 0, tiled=True)  15.9 us
    all_to_all x1, starting transfers between devices, on_device(): lax.all_to_all(send_grad.reshape(sp_count, padded, chunk), 'sp', 0, 0, ti...  13.2 us
    pallas_call x8, Pallas kernels, call(): pl.pallas_call(body, in_specs=specs, out_specs=tuple((VMEM for _ in outs)...  12.9 us
    unnamed x66, local copies, waits for them, and re-layouts  9.13 us
    all_to_all x1, waiting for transfers between devices, on_device(): lax.all_to_all(send_grad.reshape(sp_count, padded, chunk), 'sp', 0, 0, ti...  8.92 us
  transfers between devices with their start and end apart: 9, of which 6 were waited for; matrix products, arithmetic and copies ran while one was open for 9% of the time, Pallas kernels for 2%

profile of v2, /device:TPU:8, one launch (start us, length us, event | category | flops | bytes accessed | tf_op | source)
XLA Modules:
  0.0 182.4 jit_solution(3076084315910970405)
XLA Ops:
  0.7 1.1 dynamic-slice_bitcast_fusion
  1.9 2.1 %collective-permute-start = (bf16[8,128,256]{2,1,0:T(8,128)(2,1)S(1)}, bf16[8,128,256]{2,1,0:T(8,128)(2,1)S(1)}, u32[]{:S(2)}, u32[]{:S(2)}) collective-permute-start(bf16[8,128,256]{2,1,0:T(8,128)(2,1)S(1)} %pad_maximum_fusion.1), channel_id=1, source_target_pairs={{0,1},{1,0},{2,3},{3,2},{4,5},{5,4},{6,7},{7,6},{8,9},{9,8},{10,11... | collective-permute-start | bytes 1572872 | tf_op jit(solution)/shard_map/cross_send/ppermute | solution.py:279
  4.0 1.6 setup.1
  5.6 13.2 %all-to-all-start = ((bf16[32,16,128]{2,1,0:T(8,128)(2,1)}), bf16[32,16,128]{2,1,0:T(8,128)(2,1)S(1)}, u32[]{:S(2)}, u32[]{:S(2)}) async-start(bf16[32,16,128]{2,1,0:T(8,128)(2,1)} %bitcast.4), calls=%async_computation | async-start | bytes 262144 | tf_op jit(solution)/shard_map/grad_send/all_to_all | solution.py:261
  19.4 1.5 rows.1
  20.9 8.9 %all-to-all-done = bf16[32,16,128]{2,1,0:T(8,128)(2,1)S(1)} async-done(((bf16[32,16,128]{2,1,0:T(8,128)(2,1)}), bf16[32,16,128]{2,1,0:T(8,128)(2,1)S(1)}, u32[]{:S(2)}, u32[]{:S(2)}) %all-to-all-start) | async-done | bytes 131104 | tf_op jit(solution)/shard_map/grad_send/all_to_all | solution.py:261
  30.6 3.9 %all-to-all-start.1 = ((bf16[32,16,1024]{2,1,0:T(8,128)(2,1)}), bf16[32,16,1024]{2,1,0:T(8,128)(2,1)S(1)}, u32[]{:S(2)}, u32[]{:S(2)}) async-start(bf16[32,16,1024]{2,1,0:T(8,128)(2,1)} %bitcast.10), calls=%async_computation.1 | async-start | bytes 2097152 | tf_op jit(solution)/shard_map/rows_send/all_to_all | solution.py:284
  34.6 29.0 %all_gather.6.grad_ref = bf16[511,1024]{1,0:T(8,128)(2,1)S(1)} all-gather(bf16[511,128]{1,0:T(8,128)(2,1)S(1)} %bitcast.101), channel_id=1, replica_groups=mesh['sp'=32,'y'=8,'c'=2] {'y'}, dimensions={1}, use_global_device_ids=true | all-gather | bytes 1177344 | tf_op jit(solution)/shard_map/grad_gather/all_gather | solution.py:291
  63.6 1.9 %collective-permute-start.1 = (bf16[512,1024]{1,0:T(8,128)(2,1)S(1)}, bf16[512,1024]{1,0:T(8,128)(2,1)S(1)}, u32[]{:S(2)}, u32[]{:S(2)}) collective-permute-start(bf16[512,1024]{1,0:T(8,128)(2,1)S(1)} %bitcast.87), channel_id=1, source_target_pairs={{0,1},{1,0},{2,3},{3,2},{4,5},{5,4},{6,7},{7,6},{8,9},{9,8},{10,11... | collective-permute-start | bytes 3145736 | tf_op jit(solution)/shard_map/ppermute | solution.py:293
  65.5 2.4 %collective-permute-start.2 = (bf16[511,1024]{1,0:T(8,128)(2,1)S(1)}, bf16[511,1024]{1,0:T(8,128)(2,1)S(1)}, u32[]{:S(2)}, u32[]{:S(2)}) collective-permute-start(bf16[511,1024]{1,0:T(8,128)(2,1)S(1)} %all_gather.6.grad_ref), channel_id=1, source_target_pairs={{0,1},{1,0},{2,3},{3,2},{4,5},{5,4},{6,7},{7,6},{8,9},{9,8},{10,11... | collective-permute-start | bytes 3139592 | tf_op jit(solution)/shard_map/ppermute | solution.py:294
  68.0 1.0 copy-done.6
  70.2 1.5 other_half.1
  71.7 2.3 %collective-permute-start.3 = (bf16[512,256]{1,0:T(8,128)(2,1)}, bf16[512,256]{1,0:T(8,128)(2,1)}, u32[]{:S(2)}, u32[]{:S(2)}) collective-permute-start(bf16[512,256]{1,0:T(8,128)(2,1)} %get-tuple-element.31.mine_ref), channel_id=1, source_target_pairs={{0,1},{1,0},{2,3},{3,2},{4,5},{5,4},{6,7},{7,6},{8,9},{9,8},{10,11... | collective-permute-start | bytes 786440 | tf_op jit(solution)/shard_map/ppermute | solution.py:314
  75.5 1.0 copy-done.11
  76.5 1.8 input_grad.1
  78.3 1.0 copy-done.5
  79.3 6.5 %all-to-all-start.2 = ((bf16[8,512,128]{2,1,0:T(8,128)(2,1)}), bf16[8,512,128]{2,1,0:T(8,128)(2,1)S(1)}, u32[]{:S(2)}, u32[]{:S(2)}) async-start(bf16[8,512,128]{2,1,0:T(8,128)(2,1)} %copy-done.5), calls=%async_computation.2 | async-start | bytes 2097152 | tf_op jit(solution)/shard_map/all_to_all | solution.py:324
  87.1 1.2 fusion.12
  91.8 1.8 convolution_convert_fusion
  93.5 1.5 broadcast_select_fusion.1
  95.1 1.0 copy.31
  96.7 1.0 convolution_convert_fusion.2
  97.7 15.9 %all-to-all-done.2.parts_ref = bf16[8,512,128]{2,1,0:T(8,128)(2,1)S(1)} async-done(((bf16[8,512,128]{2,1,0:T(8,128)(2,1)}), bf16[8,512,128]{2,1,0:T(8,128)(2,1)S(1)}, u32[]{:S(2)}, u32[]{:S(2)}) %all-to-all-start.2) | async-done | bytes 1048608 | tf_op jit(solution)/shard_map/all_to_all | solution.py:324
  114.4 7.9 %all-to-all-start.3 = ((bf16[32,16,128]{2,1,0:T(8,128)(2,1)}), bf16[32,16,128]{2,1,0:T(8,128)(2,1)S(1)}, u32[]{:S(2)}, u32[]{:S(2)}) async-start(bf16[32,16,128]{2,1,0:T(8,128)(2,1)} %bitcast.18), calls=%async_computation.3 | async-start | bytes 262144 | tf_op jit(solution)/shard_map/all_to_all | solution.py:334
  123.6 1.2 broadcast_in_dim_reshape.3
  124.8 8.0 %all-to-all-done.3 = bf16[32,16,128]{2,1,0:T(8,128)(2,1)S(1)} async-done(((bf16[32,16,128]{2,1,0:T(8,128)(2,1)}), bf16[32,16,128]{2,1,0:T(8,128)(2,1)S(1)}, u32[]{:S(2)}, u32[]{:S(2)}) %all-to-all-start.3) | async-done | bytes 131104 | tf_op jit(solution)/shard_map/all_to_all | solution.py:334
  133.1 18.1 %all_gather.7.stream_ref = bf16[192,2048]{1,0:T(8,128)(2,1)S(1)} all-gather(bf16[192,128]{1,0:T(8,128)(2,1)S(1)} %fusion.1), channel_id=1, replica_groups=mesh['sp'=32,'y'=8,'c'=2] {'y','c'}, dimensions={1}, use_global_device_ids=true | all-gather | bytes 835584 | tf_op jit(solution)/shard_map/all_gather | solution.py:338
  151.2 3.6 %pack.1 = (bf16[192,96]{1,0:T(8,128)(2,1)S(1)}, bf16[32,88,128]{2,1,0:T(8,128)(2,1)}) custom-call(bf16[192,2048]{1,0:T(8,128)(2,1)S(1)} %all_gather.7.stream_ref, bf16[96,2048]{1,0:T(8,128)(2,1)S(1)} %copy-done.13, bf16[192,96]{1,0:T(8,128)(2,1)S(1)} %copy-done.18, bf16[192,48]{1,0:T(8,128)(2,1)S(1)} %copy-done.15, f32[192,1]{1,0:T(8,128)S(1)} %copy-done.14), custom_call_target="tpu_custom_call" | custom-call | flops 150994944 | tf_op jit(solution)/shard_map/pack/pallas_call | solution.py:29
  154.8 4.0 %all-to-all-start.4 = ((bf16[32,88,128]{2,1,0:T(8,128)(2,1)}), bf16[32,88,128]{2,1,0:T(8,128)(2,1)S(1)}, u32[]{:S(2)}, u32[]{:S(2)}) async-start(bf16[32,88,128]{2,1,0:T(8,128)(2,1)} %get-tuple-element.34), calls=%async_computation.4 | async-start | bytes 1441792 | tf_op jit(solution)/shard_map/all_to_all | solution.py:349
  158.8 1.0 slice_bitcast_fusion
  163.3 17.6 %all-to-all-done.4.got_ref = bf16[32,88,128]{2,1,0:T(8,128)(2,1)S(1)} async-done(((bf16[32,88,128]{2,1,0:T(8,128)(2,1)}), bf16[32,88,128]{2,1,0:T(8,128)(2,1)S(1)}, u32[]{:S(2)}, u32[]{:S(2)}) %all-to-all-start.4) | async-done | bytes 720928 | tf_op jit(solution)/shard_map/all_to_all | solution.py:349
  180.9 1.4 finish.1
  (94 shorter events, 15.4 us)
Async XLA Ops:
  0.6 160.8 %copy-start = (f32[1,1,48,96]{3,2,1,0:T(8,128)S(1)}, f32[1,1,48,96]{3,2,1,0:T(8,128)}, u32[]{:S(2)}) copy-start(f32[1,1,48,96]{3,2,1,0:T(8,128)} %param.27) | copy-start | bytes 55300
  1.7 17.0 %copy-start.9 = (bf16[192,2048]{1,0:T(8,128)(2,1)S(1)}, bf16[192,2048]{1,0:T(8,128)(2,1)}, u32[]{:S(2)}) copy-start(bf16[192,2048]{1,0:T(8,128)(2,1)} %input_ref.1) | copy-start | bytes 2359300
  1.8 2.2 %copy-start.16 = (bf16[192,128]{1,0:T(8,128)(2,1)S(1)}, bf16[192,128]{1,0:T(8,128)(2,1)}, u32[]{:S(2)}) copy-start(bf16[192,128]{1,0:T(8,128)(2,1)} %grad_ref.1) | copy-start | bytes 147460
  1.8 2.2 %copy-start.22 = (f32[192,2]{0,1:T(2,128)S(1)}, f32[192,2]{0,1:T(2,128)}, u32[]{:S(2)}) copy-start(f32[192,2]{0,1:T(2,128)} %param.17) | copy-start | bytes 4612
  1.8 2.1 %copy-start.21 = (s32[192,2]{0,1:T(2,128)S(1)}, s32[192,2]{0,1:T(2,128)}, u32[]{:S(2)}) copy-start(s32[192,2]{0,1:T(2,128)} %param.16) | copy-start | bytes 4612
  1.9 28.0 %collective-permute-start = (bf16[8,128,256]{2,1,0:T(8,128)(2,1)S(1)}, bf16[8,128,256]{2,1,0:T(8,128)(2,1)S(1)}, u32[]{:S(2)}, u32[]{:S(2)}) collective-permute-start(bf16[8,128,256]{2,1,0:T(8,128)(2,1)S(1)} %pad_maximum_fusion.1), channel_id=1, source_target_pairs={{0,1},{1,0},{2,3},{3,2},{4,5},{5,4},{6,7},{7,6},{8,9},{9,8},{10,11... | collective-permute-start | bytes 1572872 | tf_op jit(solution)/shard_map/cross_send/ppermute | solution.py:279
  5.6 24.2 %all-to-all-start = ((bf16[32,16,128]{2,1,0:T(8,128)(2,1)}), bf16[32,16,128]{2,1,0:T(8,128)(2,1)S(1)}, u32[]{:S(2)}, u32[]{:S(2)}) async-start(bf16[32,16,128]{2,1,0:T(8,128)(2,1)} %bitcast.4), calls=%async_computation | async-start | bytes 262144 | tf_op jit(solution)/shard_map/grad_send/all_to_all | solution.py:261
  30.6 33.0 %all-to-all-start.1 = ((bf16[32,16,1024]{2,1,0:T(8,128)(2,1)}), bf16[32,16,1024]{2,1,0:T(8,128)(2,1)S(1)}, u32[]{:S(2)}, u32[]{:S(2)}) async-start(bf16[32,16,1024]{2,1,0:T(8,128)(2,1)} %bitcast.10), calls=%async_computation.1 | async-start | bytes 2097152 | tf_op jit(solution)/shard_map/rows_send/all_to_all | solution.py:284
  34.6 33.4 %copy-start.1 = (bf16[1,2048,128]{2,1,0:T(8,128)(2,1)S(1)}, bf16[1,2048,128]{2,1,0:T(8,128)(2,1)}, u32[]{:S(2)}) copy-start(bf16[1,2048,128]{2,1,0:T(8,128)(2,1)} %param.18) | copy-start | bytes 1572868
  34.6 33.4 %copy-start.2 = (bf16[1,2048,128]{2,1,0:T(8,128)(2,1)S(1)}, bf16[1,2048,128]{2,1,0:T(8,128)(2,1)}, u32[]{:S(2)}) copy-start(bf16[1,2048,128]{2,1,0:T(8,128)(2,1)} %param.19) | copy-start | bytes 1572868
  63.6 6.6 %collective-permute-start.1 = (bf16[512,1024]{1,0:T(8,128)(2,1)S(1)}, bf16[512,1024]{1,0:T(8,128)(2,1)S(1)}, u32[]{:S(2)}, u32[]{:S(2)}) collective-permute-start(bf16[512,1024]{1,0:T(8,128)(2,1)S(1)} %bitcast.87), channel_id=1, source_target_pairs={{0,1},{1,0},{2,3},{3,2},{4,5},{5,4},{6,7},{7,6},{8,9},{9,8},{10,11... | collective-permute-start | bytes 3145736 | tf_op jit(solution)/shard_map/ppermute | solution.py:293
  65.5 4.7 %collective-permute-start.2 = (bf16[511,1024]{1,0:T(8,128)(2,1)S(1)}, bf16[511,1024]{1,0:T(8,128)(2,1)S(1)}, u32[]{:S(2)}, u32[]{:S(2)}) collective-permute-start(bf16[511,1024]{1,0:T(8,128)(2,1)S(1)} %all_gather.6.grad_ref), channel_id=1, source_target_pairs={{0,1},{1,0},{2,3},{3,2},{4,5},{5,4},{6,7},{7,6},{8,9},{9,8},{10,11... | collective-permute-start | bytes 3139592 | tf_op jit(solution)/shard_map/ppermute | solution.py:294
  68.0 1.0 copy-start.6
  69.0 1.2 copy-start.7
  70.2 1.5 copy-start.3
  70.2 1.5 copy-start.8
  71.7 3.8 %collective-permute-start.3 = (bf16[512,256]{1,0:T(8,128)(2,1)}, bf16[512,256]{1,0:T(8,128)(2,1)}, u32[]{:S(2)}, u32[]{:S(2)}) collective-permute-start(bf16[512,256]{1,0:T(8,128)(2,1)} %get-tuple-element.31.mine_ref), channel_id=1, source_target_pairs={{0,1},{1,0},{2,3},{3,2},{4,5},{5,4},{6,7},{7,6},{8,9},{9,8},{10,11... | collective-permute-start | bytes 786440 | tf_op jit(solution)/shard_map/ppermute | solution.py:314
  75.5 1.0 copy-start.11
  79.3 6.6 %copy-start.25 = (bf16[192,48]{0,1:T(8,128)(2,1)S(1)}, bf16[192,48]{0,1:T(8,128)(2,1)}, u32[]{:S(2)}) copy-start(bf16[192,48]{0,1:T(8,128)(2,1)} %param.23) | copy-start | bytes 55300
  79.3 34.3 %all-to-all-start.2 = ((bf16[8,512,128]{2,1,0:T(8,128)(2,1)}), bf16[8,512,128]{2,1,0:T(8,128)(2,1)S(1)}, u32[]{:S(2)}, u32[]{:S(2)}) async-start(bf16[8,512,128]{2,1,0:T(8,128)(2,1)} %copy-done.5), calls=%async_computation.2 | async-start | bytes 2097152 | tf_op jit(solution)/shard_map/all_to_all | solution.py:324
  95.1 1.6 copy-start.4
  114.4 7.9 %copy-start.24 = (bf16[128,1024]{1,0:T(8,128)(2,1)S(1)}, bf16[128,1024]{1,0:T(8,128)(2,1)}, u32[]{:S(2)}) copy-start(bf16[128,1024]{1,0:T(8,128)(2,1)} %convolution_convert_fusion.2) | copy-start | bytes 786436
  114.4 18.5 %all-to-all-start.3 = ((bf16[32,16,128]{2,1,0:T(8,128)(2,1)}), bf16[32,16,128]{2,1,0:T(8,128)(2,1)S(1)}, u32[]{:S(2)}, u32[]{:S(2)}) async-start(bf16[32,16,128]{2,1,0:T(8,128)(2,1)} %bitcast.18), calls=%async_computation.3 | async-start | bytes 262144 | tf_op jit(solution)/shard_map/all_to_all | solution.py:334
  123.6 9.2 %copy-start.17 = (bf16[192,128]{1,0:T(8,128)(2,1)S(1)}, bf16[192,128]{1,0:T(8,128)(2,1)}, u32[]{:S(2)}) copy-start(bf16[192,128]{1,0:T(8,128)(2,1)} %grad_ref.1) | copy-start | bytes 147460
  133.0 18.1 %copy-start.13 = (bf16[96,2048]{1,0:T(8,128)(2,1)S(1)}, bf16[96,2048]{1,0:T(8,128)(2,1)}, u32[]{:S(2)}) copy-start(bf16[96,2048]{1,0:T(8,128)(2,1)} %proj_ref.1) | copy-start | bytes 1179652
  133.1 18.1 %copy-start.14 = (f32[192,1]{1,0:T(8,128)S(1)}, f32[192,1]{1,0:T(8,128)}, u32[]{:S(2)}) copy-start(f32[192,1]{1,0:T(8,128)} %copy.34.rising_ref) | copy-start | bytes 2308
  133.1 18.1 %copy-start.15 = (bf16[192,48]{1,0:T(8,128)(2,1)S(1)}, bf16[192,48]{1,0:T(8,128)(2,1)}, u32[]{:S(2)}) copy-start(bf16[192,48]{1,0:T(8,128)(2,1)} %copy.33.query_ref) | copy-start | bytes 55300
  133.1 18.1 %copy-start.18 = (bf16[192,96]{1,0:T(8,128)(2,1)S(1)}, bf16[192,96]{1,0:T(8,128)(2,1)}, u32[]{:S(2)}) copy-start(bf16[192,96]{1,0:T(8,128)(2,1)} %kept_ref.1) | copy-start | bytes 110596
  154.8 4.0 %copy-start.23 = (bf16[8,2,128,256]{3,2,1,0:T(8,128)(2,1)S(1)}, bf16[8,2,128,256]{3,2,1,0:T(8,128)(2,1)}, u32[]{:S(2)}) copy-start(bf16[8,2,128,256]{3,2,1,0:T(8,128)(2,1)} %copy.31) | copy-start | bytes 3145732
  154.8 26.2 %all-to-all-start.4 = ((bf16[32,88,128]{2,1,0:T(8,128)(2,1)}), bf16[32,88,128]{2,1,0:T(8,128)(2,1)S(1)}, u32[]{:S(2)}, u32[]{:S(2)}) async-start(bf16[32,88,128]{2,1,0:T(8,128)(2,1)} %get-tuple-element.34), calls=%async_computation.4 | async-start | bytes 1441792 | tf_op jit(solution)/shard_map/all_to_all | solution.py:349
  158.8 1.1 copy-start.19
  162.9 18.1 %copy-start.12 = (f32[192,1]{1,0:T(8,128)S(1)}, f32[192,1]{1,0:T(8,128)}, u32[]{:S(2)}) copy-start(f32[192,1]{1,0:T(8,128)} %copy.36.tail_ref) | copy-start | bytes 2308
  (8 other events, 5.9 us)

commit v3 on v2

v3 whole, which is shorter than its diff:
```python
import functools

import jax
import jax.numpy as jnp
from jax import lax
from jax.experimental import pallas as pl
from jax.experimental.pallas import tpu as pltpu
from jax.sharding import Mesh
from jax.sharding import PartitionSpec as P

TP = ("y", "c")
F32 = jnp.float32
BF16 = jnp.bfloat16
PLAIN = (((1,), (0,)), ((), ()))
ACROSS = (((1,), (1,)), ((), ()))
ALONG = (((0,), (0,)), ((), ()))
SWAP = [(0, 1), (1, 0)]
SWAP_TYPE = BF16
VMEM = pl.BlockSpec(memory_space=pltpu.VMEM)
SMEM = pl.BlockSpec(memory_space=pltpu.SMEM)
HBM = pl.BlockSpec(memory_space=pltpu.HBM)
PLACES = {"s": SMEM, "v": VMEM, "h": HBM}


def dot(a, b, dims=PLAIN):
    return lax.dot_general(a, b, dims, preferred_element_type=F32)


def call(body, ins, outs, scratch=(), flops=0, limit=20):
    specs = [PLACES[k] for k, _ in ins]
    places = tuple(PLACES[out[2] if len(out) > 2 else "v"] for out in outs)
    arrays = [
        pltpu.with_memory_space_constraint(a, pltpu.HBM) if k == "h" else a for k, a in ins
    ]
    return pl.pallas_call(
        body,
        in_specs=specs,
        out_specs=places,
        out_shape=tuple(
            pltpu.HBM(out[0], out[1]) if len(out) > 2 else jax.ShapeDtypeStruct(out[0], out[1])
            for out in outs
        ),
        scratch_shapes=list(scratch),
        compiler_params=pltpu.CompilerParams(vmem_limit_bytes=limit << 20),
        cost_estimate=pl.CostEstimate(flops=flops, transcendentals=0, bytes_accessed=0),
    )(*arrays)


def in_three(x):
    high = x.astype(BF16)
    rest = x - high.astype(F32)
    middle = rest.astype(BF16)
    low = (rest - middle.astype(F32)).astype(BF16)
    return high, middle, low


def started(pairs, sems):
    copies = [
        pltpu.make_async_copy(source, target, sems.at[k])
        for k, (source, target) in enumerate(pairs)
    ]
    for copy in copies:
        copy.start()
    return copies


def waited(copies):
    for copy in copies:
        copy.wait()


def setup_body(
    ids_hbm, weight_hbm, grad_hbm, picker_ref, send_ref, ids_ref, weight_ref, grad_ref, sems,
    *, experts, padded,
):
    waited(
        started([(ids_hbm, ids_ref), (weight_hbm, weight_ref), (grad_hbm, grad_ref)], sems)
    )
    tokens = ids_ref.shape[1]
    slots = experts * padded
    grad = grad_ref[...].astype(F32)
    row = lax.broadcasted_iota(jnp.int32, (tokens, tokens), 0)
    col = lax.broadcasted_iota(jnp.int32, (tokens, tokens), 1)
    same = jnp.where(row == col, 1.0, 0.0).astype(BF16)
    earlier = jnp.where(row > col, 1.0, 0.0).astype(BF16)
    lines = jnp.concatenate(
        [ids_ref[...].astype(F32)] + [p.astype(F32) for p in in_three(weight_ref[...])], axis=0
    )
    columns = dot(same, lines.astype(BF16), ACROSS)
    ids = columns[:, :2]
    names = lax.broadcasted_iota(jnp.int32, (tokens, experts), 1).astype(F32)
    onehot = [jnp.where(ids[:, j : j + 1] == names, 1.0, 0.0) for j in (0, 1)]
    before = dot(earlier, (onehot[0] + onehot[1]).astype(BF16))
    spots = lax.broadcasted_iota(jnp.int32, (tokens, slots), 1)
    picker, sent = None, None
    for j in (0, 1):
        rank = jnp.sum(before * onehot[j], axis=1, keepdims=True)
        slot = (ids[:, j : j + 1] * padded + rank).astype(jnp.int32)
        hits = jnp.where(spots == slot, 1.0, 0.0).astype(BF16)
        high, middle, low = (columns[:, k + j : k + j + 1] for k in (2, 4, 6))
        weight = (high + middle) + low
        part = dot(hits, (grad * weight).astype(BF16), ALONG)
        picker = hits if picker is None else picker + hits
        sent = part if sent is None else sent + part
    picker_ref[...] = picker
    send_ref[...] = sent.astype(BF16)


def rows_body(
    core_ref, picker_ref, input_hbm, decay_hbm, send_ref, input_ref, decay_ref, sems, *, padded
):
    waited(started([(input_hbm, input_ref), (decay_hbm, decay_ref)], sems))
    rows = dot(picker_ref[...], half_columns(input_ref, core_ref[0]), ALONG)
    parts = in_three(jnp.sum(decay_ref[...], axis=1, keepdims=True))
    lane = lax.broadcasted_iota(jnp.int32, rows.shape, 1)
    row = lax.broadcasted_iota(jnp.int32, rows.shape, 0)
    extra = jnp.zeros((1, 1), F32)
    for k, part in enumerate(parts):
        extra = jnp.where(lane == k, part.astype(F32), extra)
    send_ref[...] = jnp.where((row & (padded - 1)) == padded - 1, extra, rows).astype(BF16)


def half_columns(ref, core):
    chunk = 128
    pieces = [
        ref[:, pl.ds(pl.multiple_of((2 * k + core) * chunk, chunk), chunk)]
        for k in range(ref.shape[1] // (2 * chunk))
    ]
    return jnp.concatenate(pieces, axis=1)


def prep_body(
    core_ref, gate_hbm, up_hbm, down_hbm, mine_hbm, theirs_hbm, mine_ref, theirs_ref, sems, out_sems
):
    core = core_ref[0]
    count, chunk = gate_hbm.shape[0], gate_hbm.shape[2]
    pairs = []
    for target, half in ((theirs_ref, 1 - core), (mine_ref, core)):
        pairs += [(gate_hbm.at[:, half], target.at[0]), (up_hbm.at[:, half], target.at[1])]
        for k in range(count):
            at = pl.multiple_of((2 * k + half) * chunk, chunk)
            pairs.append((down_hbm.at[:, pl.ds(at, chunk)], target.at[2, k]))
    waited(started(pairs, sems))
    waited(started([(theirs_ref, theirs_hbm), (mine_ref, mine_hbm)], out_sems))


def side_by_side(refs):
    parts = [ref[k] for ref in refs for k in (0, 1)]
    return jnp.concatenate([p.reshape(-1, p.shape[2]) for p in parts], axis=1)


def lined_up(ref):
    return jnp.concatenate([ref[2, k] for k in range(ref.shape[1])], axis=1)


def own_body(rows_ref, grad_ref, mine_hbm, cross_ref, out_ref, mine_ref, sems):
    units = mine_ref.shape[3]
    short = grad_ref.shape[0]
    copies = started(
        [(mine_hbm.at[part], mine_ref.at[part]) for part in (pl.ds(2, 1), pl.ds(0, 2))], sems
    )
    waited(copies[:1])
    downs = jnp.concatenate([lined_up(mine_ref), lined_up(cross_ref)], axis=0)
    back = dot(grad_ref[...], downs, ACROSS).astype(out_ref.dtype)
    blank = jnp.zeros((8, units), out_ref.dtype)
    for k in (0, 1):
        at = 3 * units * k + 2 * units
        out_ref[pl.ds(out_ref.shape[0] - 8, 8), at : at + units] = blank
        out_ref[pl.ds(0, short), at : at + units] = back[:, units * k : units * (k + 1)]
    waited(copies[1:])
    hidden = dot(rows_ref[...], side_by_side((mine_ref, cross_ref))).astype(out_ref.dtype)
    for k in (0, 1):
        at = 3 * units * k
        out_ref[:, at : at + 2 * units] = hidden[:, 2 * units * k : 2 * units * (k + 1)]


def units_body(
    part_ref, pair_ref, mine_hbm, cross_ref, act_hbm, both_hbm, out_hbm,
    mine_ref, act_ref, both_ref, out_ref, sems, out_sems,
):
    units = mine_ref.shape[3]
    chunk = mine_ref.shape[2]
    short = act_ref.shape[0]
    copies = started([(mine_hbm.at[pl.ds(0, 2)], mine_ref)], sems)
    for k in (0, 1):
        at, there = 3 * units * k, 3 * units * (1 - k)
        gate, up, act_grad = (
            part_ref[:, at + j * units : at + (j + 1) * units].astype(F32)
            + pair_ref[:, there + j * units : there + (j + 1) * units].astype(F32)
            for j in range(3)
        )
        sig = jax.nn.sigmoid(gate)
        swish = gate * sig
        act_ref[:, k * units : (k + 1) * units] = (swish * up).astype(BF16)[:short]
        both_ref[:, 2 * k * units : (2 * k + 1) * units] = (
            act_grad * up * sig * (1.0 + gate * (1.0 - sig))
        ).astype(BF16)
        both_ref[:, (2 * k + 1) * units : (2 * k + 2) * units] = (act_grad * swish).astype(BF16)
    count = out_ref.shape[0]
    sent = []
    for k, (source, target) in enumerate([(act_ref, act_hbm), (both_ref, both_hbm)]):
        copy = pltpu.make_async_copy(source, target, out_sems.at[count + k])
        copy.start()
        sent.append(copy)
    waited(copies)
    grads = both_ref[...]
    for k in range(0, count, 2):
        two = jnp.concatenate(
            [
                ref[j, pl.ds(k, 2)].reshape(2 * chunk, units)
                for ref in (mine_ref, cross_ref)
                for j in (0, 1)
            ],
            axis=1,
        )
        part = dot(grads, two, ACROSS).astype(BF16)
        for j in (0, 1):
            out_ref[k + j] = part[:, chunk * j : chunk * (j + 1)]
            copy = pltpu.make_async_copy(out_ref.at[k + j], out_hbm.at[k + j], out_sems.at[k + j])
            copy.start()
            sent.append(copy)
    waited(sent)


def sum_body(parts_ref, out_ref):
    total = parts_ref[0].astype(F32)
    for k in range(1, parts_ref.shape[0]):
        total = total + parts_ref[k].astype(F32)
    out_ref[...] = total.astype(BF16)


def pack_body(stream_ref, proj_ref, kept_ref, query_ref, rising_ref, ret_ref, pay_ref):
    stream = stream_ref[...]
    ret = dot(stream, proj_ref[...], ACROSS).astype(BF16)
    ret_ref[...] = ret
    inject = dot(query_ref[...] * rising_ref[...], ret)
    proj = dot(kept_ref[...], stream, ALONG)
    lanes = pay_ref.shape[2]
    width = proj.shape[0]
    fold = lanes - width
    rows = pay_ref.shape[1] - width // 2
    rest = inject.shape[0] - rows
    side = [inject[rows:, k * fold : (k + 1) * fold] for k in range(width // fold)]
    blank = jnp.zeros((rows - rest * len(side), fold), F32)
    top = jnp.concatenate(
        [inject[:rows], jnp.concatenate(side + [blank], axis=0)], axis=1
    ).astype(BF16)
    low = lax.broadcasted_iota(jnp.int32, (width // 2, lanes), 1) < lanes // 2
    for j in range(proj.shape[1] // lanes):
        tile = proj[:, j * lanes : (j + 1) * lanes]
        upper, under = tile[: width // 2], tile[width // 2 :]
        turned = [pltpu.roll(t, lanes // 2, 1) for t in (upper, under)]
        pay_ref[2 * j, :rows] = top
        pay_ref[2 * j, rows:] = jnp.where(low, upper, turned[1]).astype(BF16)
        pay_ref[2 * j + 1, :rows] = top
        pay_ref[2 * j + 1, rows:] = jnp.where(low, turned[0], under).astype(BF16)


def last_body(
    factor_ref, got_ref, keys_ref, values_ref, tail_ref, tail_row_ref, key_part_ref,
    value_part_ref, key_ref, value_ref, proj_ref,
):
    count, _, lanes = got_ref.shape
    key_dim, width = keys_ref.shape[1], values_ref.shape[1]
    rows = got_ref.shape[1] - width // 2
    fold = lanes - width
    rest = key_dim - rows
    state, total = None, None
    for m in range(count):
        part = got_ref[m, rows:].astype(F32)
        total = part if total is None else total + part
        scaled = factor_ref[m] * got_ref[m, :rows].astype(F32)
        state = scaled if state is None else state + scaled
    state = jnp.concatenate(
        [
            state[:, :width],
            jnp.concatenate(
                [state[k * rest : (k + 1) * rest, width:] for k in range(width // fold)], axis=1
            ),
        ],
        axis=0,
    ).astype(BF16)
    half = lanes // 2
    proj_ref[...] = jnp.concatenate([total[:, :half], total[:, half:]], axis=0).T
    tail = tail_ref[...]
    across = dot(state, values_ref[...], ACROSS)
    key_ref[...] = (key_part_ref[...] + tail_row_ref[...] * across).astype(BF16)
    value_ref[...] = (value_part_ref[...] + tail * dot(keys_ref[...], state)).astype(BF16)


def joined_rows(own, other, core):
    rows, cols = own.shape
    own, other = (a.reshape(8, 1, rows // 8, cols) for a in (own, other))
    first = jnp.where(core == 0, own, other)
    second = jnp.where(core == 0, other, own)
    return jnp.concatenate([first, second], axis=1).reshape(2 * rows, cols)


def joined_columns(own, other, core):
    rows, cols = own.shape
    own, other = (a.reshape(rows, 8, 1, cols // 8) for a in (own, other))
    first = jnp.where(core == 0, own, other)
    second = jnp.where(core == 0, other, own)
    return jnp.concatenate([first, second], axis=2).reshape(rows, 2 * cols)


def on_device(
    moe_input,
    out_grad,
    expert_ids,
    expert_weights,
    w_gate,
    w_up,
    w_down,
    out_proj,
    retained,
    queries,
    keys,
    values,
    log_decay,
    incoming_state,
):
    tokens, width = moe_input.shape
    sp_count = lax.axis_size("sp")
    padded = 16
    slots = sp_count * padded
    short = slots - 1
    core = lax.axis_index("c")
    block = lax.axis_index("sp")
    chunk = out_grad.shape[1]
    half = width // 2
    units = w_gate.shape[2]
    key_dim, value_dim = queries.shape[1], values.shape[1]

    core_1 = core.astype(jnp.int32).reshape(1)
    picker, send_grad = call(
        functools.partial(setup_body, experts=sp_count, padded=padded),
        [("h", expert_ids.T), ("h", expert_weights.T), ("h", out_grad)],
        [((tokens, slots), BF16), ((slots, chunk), BF16)],
        scratch=[
            pltpu.VMEM((2, tokens), jnp.int32), pltpu.VMEM((2, tokens), F32),
            pltpu.VMEM((tokens, chunk), BF16), pltpu.SemaphoreType.DMA((3,)),
        ],
    )
    gate_4 = w_gate.reshape(8, 2, chunk, units)
    up_4 = w_up.reshape(8, 2, chunk, units)
    down_2 = w_down[0]
    halves = [((3, 8, chunk, units), BF16, "h")] * 2
    mine, theirs = call(
        prep_body,
        [("s", core_1), ("h", gate_4), ("h", up_4), ("h", down_2)],
        halves,
        scratch=[
            pltpu.VMEM((3, 8, chunk, units), BF16), pltpu.VMEM((3, 8, chunk, units), BF16),
            pltpu.SemaphoreType.DMA((20,)), pltpu.SemaphoreType.DMA((2,)),
        ],
    )
    cross = lax.ppermute(theirs, "c", SWAP)
    got_grad = lax.all_to_all(send_grad.reshape(sp_count, padded, chunk), "sp", 0, 0, tiled=True)
    got_grad = got_grad.reshape(slots, chunk)[:short]

    (send_rows,) = call(
        functools.partial(rows_body, padded=padded),
        [("s", core_1), ("v", picker), ("h", moe_input), ("h", log_decay.T)],
        [((slots, half), BF16)],
        scratch=[
            pltpu.VMEM((tokens, width), BF16), pltpu.VMEM((1, tokens), F32),
            pltpu.SemaphoreType.DMA((2,)),
        ],
    )
    send_rows, got_grad = lax.optimization_barrier((send_rows, got_grad))
    send_rows = send_rows.reshape(sp_count, padded, half)
    got_rows = lax.all_to_all(send_rows, "sp", 0, 0, tiled=True)
    ends = jnp.sum(got_rows[:, padded - 1, :3].astype(F32), axis=1)
    rows_own = got_rows.reshape(slots, half)
    running = jnp.cumsum(log_decay[:, 0])
    last = running[-1]

    grad_own = lax.all_gather(got_grad, "y", axis=1, tiled=True)
    rows_own, grad_own = lax.optimization_barrier((rows_own, grad_own))
    (part,) = call(
        own_body,
        [("v", rows_own), ("v", grad_own), ("h", mine), ("v", cross)],
        [((slots, 6 * units), SWAP_TYPE)],
        scratch=[
            pltpu.VMEM(mine.shape, BF16), pltpu.SemaphoreType.DMA((2,)),
        ],
        flops=12 * slots * half * units,
    )
    pair = lax.ppermute(part, "c", SWAP)
    act, both, pieces = call(
        units_body,
        [("v", part), ("v", pair), ("h", mine), ("v", cross)],
        [
            ((short, 2 * units), BF16, "h"), ((slots, 4 * units), BF16, "h"),
            ((8, slots, chunk), BF16, "h"),
        ],
        scratch=[
            pltpu.VMEM((2, 8, chunk, units), BF16), pltpu.VMEM((short, 2 * units), BF16), pltpu.VMEM((slots, 4 * units), BF16),
            pltpu.VMEM((8, slots, chunk), BF16),
            pltpu.SemaphoreType.DMA((1,)), pltpu.SemaphoreType.DMA((10,)),
        ],
        flops=8 * slots * half * units,
    )
    pieces = lax.all_to_all(pieces, "y", 0, 0, tiled=True)

    w_parts = dot(rows_own, both, ALONG).astype(BF16)
    w_own = w_parts[:, : 2 * units]
    w_other = lax.ppermute(w_parts[:, 2 * units :], "c", SWAP)
    w_grads = joined_rows(w_own, w_other, core)
    gate_w_grad, up_w_grad = w_grads[:, :units], w_grads[:, units:]
    down_parts = dot(act, grad_own, ALONG).astype(BF16)
    down_other = lax.ppermute(down_parts[units:], "c", SWAP)
    down_grad = joined_columns(down_parts[:units], down_other, core)

    (share,) = call(sum_body, [("v", pieces)], [((slots, chunk), BF16)])
    returned = lax.all_to_all(
        share.reshape(sp_count, padded, chunk), "sp", 0, 0, tiled=True
    ).reshape(slots, chunk)
    stream_part = (out_grad.astype(F32) + dot(picker, returned)).astype(BF16)
    stream = lax.all_gather(stream_part, TP, axis=1, tiled=True)

    rising = jnp.exp(running)[:, None]
    rows = 40
    ret_grad, payload = call(
        pack_body,
        [("v", stream), ("v", out_proj), ("v", retained), ("v", queries.T), ("v", rising.T.astype(BF16))],
        [((tokens, value_dim), BF16), ((sp_count, value_dim // 2 + rows, 128), BF16)],
        flops=4 * tokens * width * value_dim,
    )
    got = lax.all_to_all(payload, "sp", 0, 0, tiled=True)

    order = jnp.arange(sp_count)
    between = (order[None, :] > block) & (order[None, :] < order[:, None])
    factors = jnp.where(
        order > block, jnp.exp(jnp.sum(jnp.where(between, ends[None, :], 0.0), axis=1)), 0.0
    )
    q, k, v, o = (a.astype(F32) for a in (queries, keys, values, ret_grad))
    place = jnp.arange(tokens)
    causal = place[:, None] >= place[None, :]
    diff = running[:, None] - running[None, :]
    decay = jnp.where(causal, jnp.exp(jnp.minimum(diff, 0.0)), 0.0)
    scores = dot(q, k, ACROSS) * decay
    prob_grad = dot(o, v, ACROSS) * decay
    tail = jnp.exp(last - running)[:, None]
    query_grad = dot(prob_grad, k) + rising * dot(o, incoming_state[0, 0], ACROSS)
    key_part = dot(q, prob_grad, ALONG)
    value_part = dot(scores, o, ALONG)
    key_grad, value_grad, out_proj_grad = call(
        last_body,
        [
            ("s", factors), ("v", got), ("v", keys), ("v", values), ("v", tail),
            ("v", tail.T), ("v", key_part), ("v", value_part),
        ],
        [
            ((key_dim, tokens), BF16), ((tokens, value_dim), BF16),
            ((width // sp_count, value_dim), F32),
        ],
    )
    return (
        gate_w_grad[None],
        up_w_grad[None],
        down_grad[None],
        out_proj_grad,
        query_grad.astype(BF16),
        key_grad.T,
        value_grad,
    )


def solution(mesh):
    torus = Mesh(mesh.devices.reshape(mesh.shape["sp"], 8, 2), ("sp", "y", "c"))
    placed = (
        P("sp", None),
        P("sp", TP),
        P("sp", None),
        P("sp", None),
        P("sp", None, TP),
        P("sp", None, TP),
        P("sp", TP, None),
        P(TP, None),
        P("sp", TP),
        P("sp", TP),
        P("sp", TP),
        P("sp", TP),
        P("sp", TP),
        P("sp", TP, None, None),
    )
    return jax.shard_map(
        on_device,
        mesh=torus,
        in_specs=placed,
        out_specs=(
            P("sp", None, TP),
            P("sp", None, TP),
            P("sp", TP, None),
            P("sp", TP),
            P("sp", TP),
            P("sp", TP),
            P("sp", TP),
        ),
        check_vma=False,
    )
```

time: 184 us -> 179 us (0.973)
  the two profiles are of different devices: /device:TPU:8 before, /device:TPU:1 now
where the time goes in v3:
time: 179 us; the launch traced here: 178 us
  waiting for transfers between devices  51.7 us (29%)
  starting transfers between devices  49 us (27%)
  blocking collectives  44.6 us (25%)
  Pallas kernels  19.5 us (11%)
  local copies, waits for them, and re-layouts  5.17 us (3%)
  matrix products  4.13 us (2%)
  other arithmetic  2.83 us (2%)
    all_gather x1, blocking collectives, on_device(): grad_own = lax.all_gather(got_grad, 'y', axis=1, tiled=True)  25.9 us
    pallas_call x8, Pallas kernels, call(): pl.pallas_call(body, in_specs=specs, out_specs=places, out_shape=tuple((p...  19.5 us
    all_gather x1, blocking collectives, on_device(): stream = lax.all_gather(stream_part, TP, axis=1, tiled=True)  18.7 us
    all_to_all x1, waiting for transfers between devices, on_device(): got = lax.all_to_all(payload, 'sp', 0, 0, tiled=True)  18.1 us
    all_to_all x1, waiting for transfers between devices, on_device(): pieces = lax.all_to_all(pieces, 'y', 0, 0, tiled=True)  17.3 us
    all_to_all x1, starting transfers between devices, on_device(): lax.all_to_all(send_grad.reshape(sp_count, padded, chunk), 'sp', 0, 0, ti...  13.7 us
    all_to_all x1, starting transfers between devices, on_device(): lax.all_to_all(share.reshape(sp_count, padded, chunk), 'sp', 0, 0, tiled=...  9.49 us
    all_to_all x1, waiting for transfers between devices, on_device(): lax.all_to_all(share.reshape(sp_count, padded, chunk), 'sp', 0, 0, tiled=...  7.97 us
  transfers between devices with their start and end apart: 9, of which 5 were waited for; matrix products, arithmetic and copies ran while one was open for 7% of the time, Pallas kernels for 3%

profile of v3, /device:TPU:1, one launch (start us, length us, event | category | flops | bytes accessed | tf_op | source)
XLA Modules:
  0.0 178.0 jit_solution(6624819268656566783)
XLA Ops:
  0.6 2.5 %shard_map.189 = (bf16[192,512]{1,0:T(8,128)(2,1)S(1)}, bf16[512,128]{1,0:T(8,128)(2,1)}) custom-call(s32[2,192]{1,0:T(2,128)} %bitcast.88, f32[2,192]{1,0:T(2,128)} %bitcast.89, bf16[192,128]{1,0:T(8,128)(2,1)} %grad_hbm.1), custom_call_target="tpu_custom_call" | custom-call | tf_op jit(solution)/shard_map/pallas_call | solution.py:35
  3.2 13.7 %all-to-all-start = ((bf16[32,16,128]{2,1,0:T(8,128)(2,1)}), bf16[32,16,128]{2,1,0:T(8,128)(2,1)S(1)}, u32[]{:S(2)}, u32[]{:S(2)}) async-start(bf16[32,16,128]{2,1,0:T(8,128)(2,1)} %bitcast.4), calls=%async_computation | async-start | bytes 262144 | tf_op jit(solution)/shard_map/all_to_all | solution.py:359
  16.9 2.6 %shard_map.190 = bf16[512,1024]{1,0:T(8,128)(2,1)} custom-call(s32[1]{0:T(128)} %bitcast.core_ref, bf16[192,512]{1,0:T(8,128)(2,1)S(1)} %get-tuple-element.23.picker_ref, bf16[192,2048]{1,0:T(8,128)(2,1)} %input_hbm.1, f32[1,192]{1,0:T(1,128)} %bitcast.86), custom_call_target="tpu_custom_call" | custom-call | tf_op jit(solution)/shard_map/pallas_call | solution.py:35
  19.5 6.7 %all-to-all-done = bf16[32,16,128]{2,1,0:T(8,128)(2,1)S(1)} async-done(((bf16[32,16,128]{2,1,0:T(8,128)(2,1)}), bf16[32,16,128]{2,1,0:T(8,128)(2,1)S(1)}, u32[]{:S(2)}, u32[]{:S(2)}) %all-to-all-start) | async-done | bytes 131104 | tf_op jit(solution)/shard_map/all_to_all | solution.py:359
  26.2 3.9 %all-to-all-start.1 = ((bf16[32,16,1024]{2,1,0:T(8,128)(2,1)}), bf16[32,16,1024]{2,1,0:T(8,128)(2,1)S(1)}, u32[]{:S(2)}, u32[]{:S(2)}) async-start(bf16[32,16,1024]{2,1,0:T(8,128)(2,1)} %bitcast.6), calls=%async_computation.1 | async-start | bytes 2097152 | tf_op jit(solution)/shard_map/all_to_all | solution.py:373
  30.2 2.7 %shard_map.191 = (bf16[3,8,128,128]{3,2,1,0:T(8,128)(2,1)}, bf16[3,8,128,128]{3,2,1,0:T(8,128)(2,1)}) custom-call(s32[1]{0:T(128)} %bitcast.core_ref, bf16[8,2,128,128]{3,2,1,0:T(8,128)(2,1)} %bitcast.82, bf16[8,2,128,128]{3,2,1,0:T(8,128)(2,1)} %bitcast.83, bf16[128,2048]{1,0:T(8,128)(2,1)} %bitcast.84), custom_call_target="tpu_custom_call" | custom-call | tf_op jit(solution)/shard_map/pallas_call | solution.py:35
  32.9 4.0 %collective-permute-start = (bf16[3,8,128,128]{3,2,1,0:T(8,128)(2,1)}, bf16[3,8,128,128]{3,2,1,0:T(8,128)(2,1)S(1)}, u32[]{:S(2)}, u32[]{:S(2)}) collective-permute-start(bf16[3,8,128,128]{3,2,1,0:T(8,128)(2,1)} %get-tuple-element.30), channel_id=1, source_target_pairs={{0,1},{1,0},{2,3},{3,2},{4,5},{5,4},{6,7},{7,6},{8,9},{9,8},{10,11... | collective-permute-start | bytes 2359304 | tf_op jit(solution)/shard_map/ppermute | solution.py:358
  36.8 25.9 %all_gather.6.grad_ref = bf16[511,1024]{1,0:T(8,128)(2,1)S(1)} all-gather(bf16[511,128]{1,0:T(8,128)(2,1)S(1)} %bitcast.81), channel_id=1, replica_groups=mesh['sp'=32,'y'=8,'c'=2] {'y'}, dimensions={1}, use_global_device_ids=true | all-gather | bytes 1177344 | tf_op jit(solution)/shard_map/all_gather | solution.py:379
  62.7 3.6 %shard_map.192.part_ref = bf16[512,768]{1,0:T(8,128)(2,1)} custom-call(bf16[512,1024]{1,0:T(8,128)(2,1)S(1)} %bitcast.71, bf16[511,1024]{1,0:T(8,128)(2,1)S(1)} %all_gather.6.grad_ref, bf16[3,8,128,128]{3,2,1,0:T(8,128)(2,1)} %get-tuple-element.29.mine_hbm, bf16[3,8,128,128]{3,2,1,0:T(8,128)(2,1)S(1)} %collective-permute-done.cross_ref), custom_call_target="tpu_custom_call" | custom-call | flops 805306368 | tf_op jit(solution)/shard_map/pallas_call | solution.py:35
  66.3 5.9 %collective-permute-start.1 = (bf16[512,768]{1,0:T(8,128)(2,1)}, bf16[512,768]{1,0:T(8,128)(2,1)}, u32[]{:S(2)}, u32[]{:S(2)}) collective-permute-start(bf16[512,768]{1,0:T(8,128)(2,1)} %shard_map.192.part_ref), channel_id=1, source_target_pairs={{0,1},{1,0},{2,3},{3,2},{4,5},{5,4},{6,7},{7,6},{8,9},{9,8},{10,11... | collective-permute-start | bytes 2359304 | tf_op jit(solution)/shard_map/ppermute | solution.py:390
  72.8 1.7 collective-permute-done.1.pair_ref
  74.5 4.1 %shard_map.193 = (bf16[511,256]{1,0:T(8,128)(2,1)}, bf16[512,512]{1,0:T(8,128)(2,1)}, bf16[8,512,128]{2,1,0:T(8,128)(2,1)}) custom-call(bf16[512,768]{1,0:T(8,128)(2,1)} %shard_map.192.part_ref, bf16[512,768]{1,0:T(8,128)(2,1)} %collective-permute-done.1.pair_ref, bf16[3,8,128,128]{3,2,1,0:T(8,128)(2,1)} %get-tuple-element.29.mine_hbm, ...), custom_call_target="tpu_custom_call" | custom-call | flops 536870912 | tf_op jit(solution)/shard_map/pallas_call | solution.py:35
  78.6 3.6 %all-to-all-start.2 = ((bf16[8,512,128]{2,1,0:T(8,128)(2,1)}), bf16[8,512,128]{2,1,0:T(8,128)(2,1)S(1)}, u32[]{:S(2)}, u32[]{:S(2)}) async-start(bf16[8,512,128]{2,1,0:T(8,128)(2,1)} %get-tuple-element.33), calls=%async_computation.2 | async-start | bytes 2097152 | tf_op jit(solution)/shard_map/all_to_all | solution.py:405
  84.2 1.5 convolution_convert_fusion.1
  85.7 2.6 %collective-permute-start.3 = (bf16[128,1024]{1,0:T(8,128)(2,1)S(1)}, bf16[128,1024]{1,0:T(8,128)(2,1)S(1)}, u32[]{:S(2)}, u32[]{:S(2)}) collective-permute-start(bf16[128,1024]{1,0:T(8,128)(2,1)S(1)} %slice.56), channel_id=1, source_target_pairs={{0,1},{1,0},{2,3},{3,2},{4,5},{5,4},{6,7},{7,6},{8,9},{9,8},{10,11... | collective-permute-start | bytes 786440 | tf_op jit(solution)/shard_map/ppermute | solution.py:413
  88.3 0.8 convolution_convert_fusion
  89.1 0.9 slice.52
  90.0 1.9 %collective-permute-start.2 = (bf16[1024,256]{1,0:T(8,128)(2,1)}, bf16[1024,256]{1,0:T(8,128)(2,1)}, u32[]{:S(2)}, u32[]{:S(2)}) collective-permute-start(bf16[1024,256]{1,0:T(8,128)(2,1)} %slice.52), channel_id=1, source_target_pairs={{0,1},{1,0},{2,3},{3,2},{4,5},{5,4},{6,7},{7,6},{8,9},{9,8},{10,11... | collective-permute-start | bytes 1572872 | tf_op jit(solution)/shard_map/ppermute | solution.py:409
  92.1 0.8 copy.29
  92.9 1.2 broadcast_in_dim_reshape.3
  94.1 17.3 %all-to-all-done.2.parts_ref = bf16[8,512,128]{2,1,0:T(8,128)(2,1)S(1)} async-done(((bf16[8,512,128]{2,1,0:T(8,128)(2,1)}), bf16[8,512,128]{2,1,0:T(8,128)(2,1)S(1)}, u32[]{:S(2)}, u32[]{:S(2)}) %all-to-all-start.2) | async-done | bytes 1048608 | tf_op jit(solution)/shard_map/all_to_all | solution.py:405
  111.4 0.8 shard_map.194
  112.2 9.5 %all-to-all-start.3 = ((bf16[32,16,128]{2,1,0:T(8,128)(2,1)}), bf16[32,16,128]{2,1,0:T(8,128)(2,1)S(1)}, u32[]{:S(2)}, u32[]{:S(2)}) async-start(bf16[32,16,128]{2,1,0:T(8,128)(2,1)} %bitcast.16), calls=%async_computation.3 | async-start | bytes 262144 | tf_op jit(solution)/shard_map/all_to_all | solution.py:417
  121.7 1.1 broadcast_select_fusion.1
  123.1 8.0 %all-to-all-done.3 = bf16[32,16,128]{2,1,0:T(8,128)(2,1)S(1)} async-done(((bf16[32,16,128]{2,1,0:T(8,128)(2,1)}), bf16[32,16,128]{2,1,0:T(8,128)(2,1)S(1)}, u32[]{:S(2)}, u32[]{:S(2)}) %all-to-all-start.3) | async-done | bytes 131104 | tf_op jit(solution)/shard_map/all_to_all | solution.py:417
  131.2 18.7 %all_gather.7.stream_ref = bf16[192,2048]{1,0:T(8,128)(2,1)S(1)} all-gather(bf16[192,128]{1,0:T(8,128)(2,1)S(1)} %fusion.1), channel_id=1, replica_groups=mesh['sp'=32,'y'=8,'c'=2] {'y','c'}, dimensions={1}, use_global_device_ids=true | all-gather | bytes 835584 | tf_op jit(solution)/shard_map/all_gather | solution.py:421
  150.0 1.8 %shard_map.195 = (bf16[192,96]{1,0:T(8,128)(2,1)S(1)}, bf16[32,88,128]{2,1,0:T(8,128)(2,1)}) custom-call(bf16[192,2048]{1,0:T(8,128)(2,1)S(1)} %all_gather.7.stream_ref, bf16[96,2048]{1,0:T(8,128)(2,1)S(1)} %copy-done.1, bf16[192,96]{1,0:T(8,128)(2,1)S(1)} %copy-done.3, bf16[48,192]{1,0:T(8,128)(2,1)S(1)} %bitcast.73, ...), custom_call_target="tpu_custom_call" | custom-call | flops 150994944 | tf_op jit(solution)/shard_map/pallas_call | solution.py:35
  151.7 3.9 %all-to-all-start.4 = ((bf16[32,88,128]{2,1,0:T(8,128)(2,1)}), bf16[32,88,128]{2,1,0:T(8,128)(2,1)S(1)}, u32[]{:S(2)}, u32[]{:S(2)}) async-start(bf16[32,88,128]{2,1,0:T(8,128)(2,1)} %get-tuple-element.34), calls=%async_computation.4 | async-start | bytes 1441792 | tf_op jit(solution)/shard_map/all_to_all | solution.py:431
  155.7 1.0 slice_bitcast_fusion
  157.0 0.8 fusion.3
  158.4 18.1 %all-to-all-done.4.got_ref = bf16[32,88,128]{2,1,0:T(8,128)(2,1)S(1)} async-done(((bf16[32,88,128]{2,1,0:T(8,128)(2,1)}), bf16[32,88,128]{2,1,0:T(8,128)(2,1)S(1)}, u32[]{:S(2)}, u32[]{:S(2)}) %all-to-all-start.4) | async-done | bytes 720928 | tf_op jit(solution)/shard_map/all_to_all | solution.py:431
  176.5 1.5 shard_map.196
  (53 shorter events, 4.1 us)
Async XLA Ops:
  0.6 156.4 %copy-start = (f32[1,1,48,96]{3,2,1,0:T(8,128)S(1)}, f32[1,1,48,96]{3,2,1,0:T(8,128)}, u32[]{:S(2)}) copy-start(f32[1,1,48,96]{3,2,1,0:T(8,128)} %param.27) | copy-start | bytes 55300
  3.2 23.1 %all-to-all-start = ((bf16[32,16,128]{2,1,0:T(8,128)(2,1)}), bf16[32,16,128]{2,1,0:T(8,128)(2,1)S(1)}, u32[]{:S(2)}, u32[]{:S(2)}) async-start(bf16[32,16,128]{2,1,0:T(8,128)(2,1)} %bitcast.4), calls=%async_computation | async-start | bytes 262144 | tf_op jit(solution)/shard_map/all_to_all | solution.py:359
  26.2 36.5 %all-to-all-start.1 = ((bf16[32,16,1024]{2,1,0:T(8,128)(2,1)}), bf16[32,16,1024]{2,1,0:T(8,128)(2,1)S(1)}, u32[]{:S(2)}, u32[]{:S(2)}) async-start(bf16[32,16,1024]{2,1,0:T(8,128)(2,1)} %bitcast.6), calls=%async_computation.1 | async-start | bytes 2097152 | tf_op jit(solution)/shard_map/all_to_all | solution.py:373
  32.9 29.9 %collective-permute-start = (bf16[3,8,128,128]{3,2,1,0:T(8,128)(2,1)}, bf16[3,8,128,128]{3,2,1,0:T(8,128)(2,1)S(1)}, u32[]{:S(2)}, u32[]{:S(2)}) collective-permute-start(bf16[3,8,128,128]{3,2,1,0:T(8,128)(2,1)} %get-tuple-element.30), channel_id=1, source_target_pairs={{0,1},{1,0},{2,3},{3,2},{4,5},{5,4},{6,7},{7,6},{8,9},{9,8},{10,11... | collective-permute-start | bytes 2359304 | tf_op jit(solution)/shard_map/ppermute | solution.py:358
  62.7 9.5 %copy-start.9 = (f32[192,1]{0,1:T(1,128)S(1)}, f32[192,1]{0,1:T(1,128)}, u32[]{:S(2)}) copy-start(f32[192,1]{0,1:T(1,128)} %param.26) | copy-start | bytes 2308
  66.3 8.2 %collective-permute-start.1 = (bf16[512,768]{1,0:T(8,128)(2,1)}, bf16[512,768]{1,0:T(8,128)(2,1)}, u32[]{:S(2)}, u32[]{:S(2)}) collective-permute-start(bf16[512,768]{1,0:T(8,128)(2,1)} %shard_map.192.part_ref), channel_id=1, source_target_pairs={{0,1},{1,0},{2,3},{3,2},{4,5},{5,4},{6,7},{7,6},{8,9},{9,8},{10,11... | collective-permute-start | bytes 2359304 | tf_op jit(solution)/shard_map/ppermute | solution.py:390
  78.6 5.0 %copy-start.8 = (bf16[192,48]{0,1:T(8,128)(2,1)S(1)}, bf16[192,48]{0,1:T(8,128)(2,1)}, u32[]{:S(2)}) copy-start(bf16[192,48]{0,1:T(8,128)(2,1)} %param.24) | copy-start | bytes 55300
  78.6 32.8 %all-to-all-start.2 = ((bf16[8,512,128]{2,1,0:T(8,128)(2,1)}), bf16[8,512,128]{2,1,0:T(8,128)(2,1)S(1)}, u32[]{:S(2)}, u32[]{:S(2)}) async-start(bf16[8,512,128]{2,1,0:T(8,128)(2,1)} %get-tuple-element.33), calls=%async_computation.2 | async-start | bytes 2097152 | tf_op jit(solution)/shard_map/all_to_all | solution.py:405
  84.2 4.1 %copy-start.10 = (bf16[512,512]{1,0:T(8,128)(2,1)S(1)}, bf16[512,512]{1,0:T(8,128)(2,1)}, u32[]{:S(2)}) copy-start(bf16[512,512]{1,0:T(8,128)(2,1)} %get-tuple-element.31) | copy-start | bytes 1572868
  85.7 6.2 %collective-permute-start.3 = (bf16[128,1024]{1,0:T(8,128)(2,1)S(1)}, bf16[128,1024]{1,0:T(8,128)(2,1)S(1)}, u32[]{:S(2)}, u32[]{:S(2)}) collective-permute-start(bf16[128,1024]{1,0:T(8,128)(2,1)S(1)} %slice.56), channel_id=1, source_target_pairs={{0,1},{1,0},{2,3},{3,2},{4,5},{5,4},{6,7},{7,6},{8,9},{9,8},{10,11... | collective-permute-start | bytes 786440 | tf_op jit(solution)/shard_map/ppermute | solution.py:413
  89.1 2.9 %copy-start.5 = (bf16[1024,512]{1,0:T(8,128)(2,1)}, bf16[1024,512]{1,0:T(8,128)(2,1)S(1)}, u32[]{:S(2)}) copy-start(bf16[1024,512]{1,0:T(8,128)(2,1)S(1)} %convolution_convert_fusion) | copy-start | bytes 3145732
  90.0 31.7 %collective-permute-start.2 = (bf16[1024,256]{1,0:T(8,128)(2,1)}, bf16[1024,256]{1,0:T(8,128)(2,1)}, u32[]{:S(2)}, u32[]{:S(2)}) collective-permute-start(bf16[1024,256]{1,0:T(8,128)(2,1)} %slice.52), channel_id=1, source_target_pairs={{0,1},{1,0},{2,3},{3,2},{4,5},{5,4},{6,7},{7,6},{8,9},{9,8},{10,11... | collective-permute-start | bytes 1572872 | tf_op jit(solution)/shard_map/ppermute | solution.py:409
  94.1 27.6 %copy-start.6 = (bf16[1024,512]{1,0:T(8,128)(2,1)S(1)}, bf16[1024,512]{1,0:T(8,128)(2,1)}, u32[]{:S(2)}) copy-start(bf16[1024,512]{1,0:T(8,128)(2,1)} %copy-done.5) | copy-start | bytes 3145732
  112.2 18.8 %all-to-all-start.3 = ((bf16[32,16,128]{2,1,0:T(8,128)(2,1)}), bf16[32,16,128]{2,1,0:T(8,128)(2,1)S(1)}, u32[]{:S(2)}, u32[]{:S(2)}) async-start(bf16[32,16,128]{2,1,0:T(8,128)(2,1)} %bitcast.16), calls=%async_computation.3 | async-start | bytes 262144 | tf_op jit(solution)/shard_map/all_to_all | solution.py:417
  122.9 8.1 %copy-start.7 = (bf16[192,128]{1,0:T(8,128)(2,1)S(1)}, bf16[192,128]{1,0:T(8,128)(2,1)}, u32[]{:S(2)}) copy-start(bf16[192,128]{1,0:T(8,128)(2,1)} %grad_hbm.1) | copy-start | bytes 147460
  123.0 26.9 %copy-start.1 = (bf16[96,2048]{1,0:T(8,128)(2,1)S(1)}, bf16[96,2048]{1,0:T(8,128)(2,1)}, u32[]{:S(2)}) copy-start(bf16[96,2048]{1,0:T(8,128)(2,1)} %proj_ref.1) | copy-start | bytes 1179652
  123.0 26.9 %copy-start.2 = (bf16[192,48]{0,1:T(8,128)(2,1)S(1)}, bf16[192,48]{0,1:T(8,128)(2,1)}, u32[]{:S(2)}) copy-start(bf16[192,48]{0,1:T(8,128)(2,1)} %param.23) | copy-start | bytes 55300
  123.0 26.9 %copy-start.3 = (bf16[192,96]{1,0:T(8,128)(2,1)S(1)}, bf16[192,96]{1,0:T(8,128)(2,1)}, u32[]{:S(2)}) copy-start(bf16[192,96]{1,0:T(8,128)(2,1)} %kept_ref.1) | copy-start | bytes 110596
  151.7 24.8 %all-to-all-start.4 = ((bf16[32,88,128]{2,1,0:T(8,128)(2,1)}), bf16[32,88,128]{2,1,0:T(8,128)(2,1)S(1)}, u32[]{:S(2)}, u32[]{:S(2)}) async-start(bf16[32,88,128]{2,1,0:T(8,128)(2,1)} %get-tuple-element.34), calls=%async_computation.4 | async-start | bytes 1441792 | tf_op jit(solution)/shard_map/all_to_all | solution.py:431
  155.6 1.1 copy-start.4

commit v4 on v3

--- a/solution.py
+++ b/solution.py
@@ -159,6 +159,8 @@
     copies = started(
         [(mine_hbm.at[part], mine_ref.at[part]) for part in (pl.ds(2, 1), pl.ds(0, 2))], sems
     )
+    crossed = dot(rows_ref[...], side_by_side((cross_ref,))).astype(out_ref.dtype)
+    out_ref[:, 3 * units : 5 * units] = crossed
     waited(copies[:1])
     downs = jnp.concatenate([lined_up(mine_ref), lined_up(cross_ref)], axis=0)
     back = dot(grad_ref[...], downs, ACROSS).astype(out_ref.dtype)
@@ -168,10 +170,7 @@
         out_ref[pl.ds(out_ref.shape[0] - 8, 8), at : at + units] = blank
         out_ref[pl.ds(0, short), at : at + units] = back[:, units * k : units * (k + 1)]
     waited(copies[1:])
-    hidden = dot(rows_ref[...], side_by_side((mine_ref, cross_ref))).astype(out_ref.dtype)
-    for k in (0, 1):
-        at = 3 * units * k
-        out_ref[:, at : at + 2 * units] = hidden[:, 2 * units * k : 2 * units * (k + 1)]
+    out_ref[:, : 2 * units] = dot(rows_ref[...], side_by_side((mine_ref,))).astype(out_ref.dtype)
 
 
 def units_body(
@@ -215,17 +214,18 @@
         )
         part = dot(grads, two, ACROSS).astype(BF16)
         for j in (0, 1):
-            out_ref[k + j] = part[:, chunk * j : chunk * (j + 1)]
-            copy = pltpu.make_async_copy(out_ref.at[k + j], out_hbm.at[k + j], out_sems.at[k + j])
+            piece = part[:, chunk * j : chunk * (j + 1)]
+            out_ref[k + j] = piece.reshape(out_ref.shape[1:])
+            copy = pltpu.make_async_copy(out_ref.at[k + j], out_hbm.at[:, k + j], out_sems.at[k + j])
             copy.start()
             sent.append(copy)
     waited(sent)
 
 
 def sum_body(parts_ref, out_ref):
-    total = parts_ref[0].astype(F32)
-    for k in range(1, parts_ref.shape[0]):
-        total = total + parts_ref[k].astype(F32)
+    total = parts_ref[:, 0].astype(F32)
+    for k in range(1, parts_ref.shape[1]):
+        total = total + parts_ref[:, k].astype(F32)
     out_ref[...] = total.astype(BF16)
 
 
@@ -393,16 +393,18 @@
         [("v", part), ("v", pair), ("h", mine), ("v", cross)],
         [
             ((short, 2 * units), BF16, "h"), ((slots, 4 * units), BF16, "h"),
-            ((8, slots, chunk), BF16, "h"),
+            ((sp_count, 8, padded, chunk), BF16, "h"),
         ],
         scratch=[
             pltpu.VMEM((2, 8, chunk, units), BF16), pltpu.VMEM((short, 2 * units), BF16), pltpu.VMEM((slots, 4 * units), BF16),
-            pltpu.VMEM((8, slots, chunk), BF16),
+            pltpu.VMEM((8, sp_count, padded, chunk), BF16),
             pltpu.SemaphoreType.DMA((1,)), pltpu.SemaphoreType.DMA((10,)),
         ],
         flops=8 * slots * half * units,
     )
-    pieces = lax.all_to_all(pieces, "y", 0, 0, tiled=True)
+    pieces = pieces.reshape(sp_count * 8, padded, chunk)
+    pieces = lax.all_to_all(pieces, ("sp", "y"), 0, 0, tiled=True)
+    pieces = pieces.reshape(sp_count, 8, padded, chunk)
 
     w_parts = dot(rows_own, both, ALONG).astype(BF16)
     w_own = w_parts[:, : 2 * units]
@@ -413,10 +415,8 @@
     down_other = lax.ppermute(down_parts[units:], "c", SWAP)
     down_grad = joined_columns(down_parts[:units], down_other, core)
 
-    (share,) = call(sum_body, [("v", pieces)], [((slots, chunk), BF16)])
-    returned = lax.all_to_all(
-        share.reshape(sp_count, padded, chunk), "sp", 0, 0, tiled=True
-    ).reshape(slots, chunk)
+    (returned,) = call(sum_body, [("v", pieces)], [((sp_count, padded, chunk), BF16)])
+    returned = returned.reshape(slots, chunk)
     stream_part = (out_grad.astype(F32) + dot(picker, returned)).astype(BF16)
     stream = lax.all_gather(stream_part, TP, axis=1, tiled=True)
 

time: 179 us -> 174 us (0.972)
  the two profiles are of different devices: /device:TPU:1 before, /device:TPU:8 now
where the time goes in v4:
time: 174 us; the launch traced here: 173 us
  waiting for transfers between devices  48.8 us (28%)
  blocking collectives  46.8 us (27%)
  starting transfers between devices  45.2 us (26%)
  Pallas kernels  18.7 us (11%)
  local copies, waits for them, and re-layouts  5.18 us (3%)
  matrix products  4.12 us (2%)
  other arithmetic  2.83 us (2%)
    all_gather x1, blocking collectives, on_device(): grad_own = lax.all_gather(got_grad, 'y', axis=1, tiled=True)  29.2 us
    all_to_all x1, waiting for transfers between devices, on_device(): pieces = lax.all_to_all(pieces, ('sp', 'y'), 0, 0, tiled=True)  20.2 us
    all_to_all x1, waiting for transfers between devices, on_device(): got = lax.all_to_all(payload, 'sp', 0, 0, tiled=True)  19.4 us
    pallas_call x8, Pallas kernels, call(): pl.pallas_call(body, in_specs=specs, out_specs=places, out_shape=tuple((p...  18.7 us
    all_gather x1, blocking collectives, on_device(): stream = lax.all_gather(stream_part, TP, axis=1, tiled=True)  17.6 us
    all_to_all x1, starting transfers between devices, on_device(): pieces = lax.all_to_all(pieces, ('sp', 'y'), 0, 0, tiled=True)  15.3 us
    all_to_all x1, starting transfers between devices, on_device(): lax.all_to_all(send_grad.reshape(sp_count, padded, chunk), 'sp', 0, 0, ti...  13.2 us
    all_to_all x1, waiting for transfers between devices, on_device(): lax.all_to_all(send_grad.reshape(sp_count, padded, chunk), 'sp', 0, 0, ti...  7.83 us
  transfers between devices with their start and end apart: 8, of which 4 were waited for; matrix products, arithmetic and copies ran while one was open for 7% of the time, Pallas kernels for 3%

profile of v4, /device:TPU:8, one launch (start us, length us, event | category | flops | bytes accessed | tf_op | source)
XLA Modules:
  0.0 172.7 jit_solution(10542084002299899173)
XLA Ops:
  0.6 2.5 %shard_map.189 = (bf16[192,512]{1,0:T(8,128)(2,1)S(1)}, bf16[512,128]{1,0:T(8,128)(2,1)}) custom-call(s32[2,192]{1,0:T(2,128)} %bitcast.91, f32[2,192]{1,0:T(2,128)} %bitcast.92, bf16[192,128]{1,0:T(8,128)(2,1)} %grad_hbm.1), custom_call_target="tpu_custom_call" | custom-call | tf_op jit(solution)/shard_map/pallas_call | solution.py:35
  3.2 13.2 %all-to-all-start = ((bf16[32,16,128]{2,1,0:T(8,128)(2,1)}), bf16[32,16,128]{2,1,0:T(8,128)(2,1)S(1)}, u32[]{:S(2)}, u32[]{:S(2)}) async-start(bf16[32,16,128]{2,1,0:T(8,128)(2,1)} %bitcast.4), calls=%async_computation | async-start | bytes 262144 | tf_op jit(solution)/shard_map/all_to_all | solution.py:359
  16.3 2.6 %shard_map.190 = bf16[512,1024]{1,0:T(8,128)(2,1)} custom-call(s32[1]{0:T(128)} %bitcast.core_ref, bf16[192,512]{1,0:T(8,128)(2,1)S(1)} %get-tuple-element.23.picker_ref, bf16[192,2048]{1,0:T(8,128)(2,1)} %input_hbm.1, f32[1,192]{1,0:T(1,128)} %bitcast.89), custom_call_target="tpu_custom_call" | custom-call | tf_op jit(solution)/shard_map/pallas_call | solution.py:35
  19.0 7.8 %all-to-all-done = bf16[32,16,128]{2,1,0:T(8,128)(2,1)S(1)} async-done(((bf16[32,16,128]{2,1,0:T(8,128)(2,1)}), bf16[32,16,128]{2,1,0:T(8,128)(2,1)S(1)}, u32[]{:S(2)}, u32[]{:S(2)}) %all-to-all-start) | async-done | bytes 131104 | tf_op jit(solution)/shard_map/all_to_all | solution.py:359
  26.8 3.9 %all-to-all-start.1 = ((bf16[32,16,1024]{2,1,0:T(8,128)(2,1)}), bf16[32,16,1024]{2,1,0:T(8,128)(2,1)S(1)}, u32[]{:S(2)}, u32[]{:S(2)}) async-start(bf16[32,16,1024]{2,1,0:T(8,128)(2,1)} %bitcast.6), calls=%async_computation.1 | async-start | bytes 2097152 | tf_op jit(solution)/shard_map/all_to_all | solution.py:373
  30.7 2.7 %shard_map.191 = (bf16[3,8,128,128]{3,2,1,0:T(8,128)(2,1)}, bf16[3,8,128,128]{3,2,1,0:T(8,128)(2,1)}) custom-call(s32[1]{0:T(128)} %bitcast.core_ref, bf16[8,2,128,128]{3,2,1,0:T(8,128)(2,1)} %bitcast.86, bf16[8,2,128,128]{3,2,1,0:T(8,128)(2,1)} %bitcast.87, bf16[128,2048]{1,0:T(8,128)(2,1)} %bitcast.88), custom_call_target="tpu_custom_call" | custom-call | tf_op jit(solution)/shard_map/pallas_call | solution.py:35
  33.4 1.9 %collective-permute-start = (bf16[3,8,128,128]{3,2,1,0:T(8,128)(2,1)}, bf16[3,8,128,128]{3,2,1,0:T(8,128)(2,1)S(1)}, u32[]{:S(2)}, u32[]{:S(2)}) collective-permute-start(bf16[3,8,128,128]{3,2,1,0:T(8,128)(2,1)} %get-tuple-element.30), channel_id=1, source_target_pairs={{0,1},{1,0},{2,3},{3,2},{4,5},{5,4},{6,7},{7,6},{8,9},{9,8},{10,11... | collective-permute-start | bytes 2359304 | tf_op jit(solution)/shard_map/ppermute | solution.py:358
  35.4 29.2 %all_gather.6.grad_ref = bf16[511,1024]{1,0:T(8,128)(2,1)S(1)} all-gather(bf16[511,128]{1,0:T(8,128)(2,1)S(1)} %bitcast.85), channel_id=1, replica_groups=mesh['sp'=32,'y'=8,'c'=2] {'y'}, dimensions={1}, use_global_device_ids=true | all-gather | bytes 1177344 | tf_op jit(solution)/shard_map/all_gather | solution.py:379
  64.6 3.4 %shard_map.192.part_ref = bf16[512,768]{1,0:T(8,128)(2,1)} custom-call(bf16[512,1024]{1,0:T(8,128)(2,1)S(1)} %bitcast.72, bf16[511,1024]{1,0:T(8,128)(2,1)S(1)} %all_gather.6.grad_ref, bf16[3,8,128,128]{3,2,1,0:T(8,128)(2,1)} %get-tuple-element.29.mine_hbm, bf16[3,8,128,128]{3,2,1,0:T(8,128)(2,1)S(1)} %collective-permute-done.cross_ref), custom_call_target="tpu_custom_call" | custom-call | flops 805306368 | tf_op jit(solution)/shard_map/pallas_call | solution.py:35
  68.0 1.9 %collective-permute-start.1 = (bf16[512,768]{1,0:T(8,128)(2,1)}, bf16[512,768]{1,0:T(8,128)(2,1)}, u32[]{:S(2)}, u32[]{:S(2)}) collective-permute-start(bf16[512,768]{1,0:T(8,128)(2,1)} %shard_map.192.part_ref), channel_id=1, source_target_pairs={{0,1},{1,0},{2,3},{3,2},{4,5},{5,4},{6,7},{7,6},{8,9},{9,8},{10,11... | collective-permute-start | bytes 2359304 | tf_op jit(solution)/shard_map/ppermute | solution.py:390
  70.6 0.6 slice.49
  71.2 1.4 collective-permute-done.1.pair_ref
  72.6 4.1 %shard_map.193 = (bf16[511,256]{1,0:T(8,128)(2,1)}, bf16[512,512]{1,0:T(8,128)(2,1)}, bf16[32,8,16,128]{3,2,1,0:T(8,128)(2,1)}) custom-call(bf16[512,768]{1,0:T(8,128)(2,1)} %shard_map.192.part_ref, bf16[512,768]{1,0:T(8,128)(2,1)} %collective-permute-done.1.pair_ref, bf16[3,8,128,128]{3,2,1,0:T(8,128)(2,1)} %get-tuple-element.29.mine_hbm, ...), custom_call_target="tpu_custom_call" | custom-call | flops 536870912 | tf_op jit(solution)/shard_map/pallas_call | solution.py:35
  76.7 15.3 %all-to-all-start.2 = ((bf16[256,16,128]{2,1,0:T(8,128)(2,1)}), bf16[256,16,128]{2,1,0:T(8,128)(2,1)S(1)}, u32[]{:S(2)}, u32[]{:S(2)}) async-start(bf16[256,16,128]{2,1,0:T(8,128)(2,1)} %bitcast.82), calls=%async_computation.2 | async-start | bytes 2097152 | tf_op jit(solution)/shard_map/all_to_all | solution.py:406
  92.1 0.7 slice_exponential_fusion
  93.5 1.5 convolution_convert_fusion.1
  95.0 1.9 %collective-permute-start.3 = (bf16[128,1024]{1,0:T(8,128)(2,1)S(1)}, bf16[128,1024]{1,0:T(8,128)(2,1)S(1)}, u32[]{:S(2)}, u32[]{:S(2)}) collective-permute-start(bf16[128,1024]{1,0:T(8,128)(2,1)S(1)} %slice.56), channel_id=1, source_target_pairs={{0,1},{1,0},{2,3},{3,2},{4,5},{5,4},{6,7},{7,6},{8,9},{9,8},{10,11... | collective-permute-start | bytes 786440 | tf_op jit(solution)/shard_map/ppermute | solution.py:415
  96.9 0.7 convolution_convert_fusion
  97.6 0.9 slice.52
  98.6 2.6 %collective-permute-start.2 = (bf16[1024,256]{1,0:T(8,128)(2,1)}, bf16[1024,256]{1,0:T(8,128)(2,1)S(1)}, u32[]{:S(2)}, u32[]{:S(2)}) collective-permute-start(bf16[1024,256]{1,0:T(8,128)(2,1)} %slice.52), channel_id=1, source_target_pairs={{0,1},{1,0},{2,3},{3,2},{4,5},{5,4},{6,7},{7,6},{8,9},{9,8},{10,11... | collective-permute-start | bytes 1572872 | tf_op jit(solution)/shard_map/ppermute | solution.py:411
  101.4 0.8 copy.29
  102.2 1.2 broadcast_in_dim_reshape.3
  103.4 1.1 broadcast_select_fusion.1
  104.7 20.2 %all-to-all-done.2 = bf16[256,16,128]{2,1,0:T(8,128)(2,1)S(1)} async-done(((bf16[256,16,128]{2,1,0:T(8,128)(2,1)}), bf16[256,16,128]{2,1,0:T(8,128)(2,1)S(1)}, u32[]{:S(2)}, u32[]{:S(2)}) %all-to-all-start.2) | async-done | bytes 1048608 | tf_op jit(solution)/shard_map/all_to_all | solution.py:406
  125.3 17.6 %all_gather.7.stream_ref = bf16[192,2048]{1,0:T(8,128)(2,1)S(1)} all-gather(bf16[192,128]{1,0:T(8,128)(2,1)S(1)} %fusion.1), channel_id=1, replica_groups=mesh['sp'=32,'y'=8,'c'=2] {'y','c'}, dimensions={1}, use_global_device_ids=true | all-gather | bytes 835584 | tf_op jit(solution)/shard_map/all_gather | solution.py:421
  142.9 1.8 %shard_map.195 = (bf16[192,96]{1,0:T(8,128)(2,1)S(1)}, bf16[32,88,128]{2,1,0:T(8,128)(2,1)}) custom-call(bf16[192,2048]{1,0:T(8,128)(2,1)S(1)} %all_gather.7.stream_ref, bf16[96,2048]{1,0:T(8,128)(2,1)S(1)} %copy-done.1, bf16[192,96]{1,0:T(8,128)(2,1)S(1)} %copy-done.3, bf16[48,192]{1,0:T(8,128)(2,1)S(1)} %bitcast.76, ...), custom_call_target="tpu_custom_call" | custom-call | flops 150994944 | tf_op jit(solution)/shard_map/pallas_call | solution.py:35
  144.7 4.4 %all-to-all-start.3 = ((bf16[32,88,128]{2,1,0:T(8,128)(2,1)}), bf16[32,88,128]{2,1,0:T(8,128)(2,1)S(1)}, u32[]{:S(2)}, u32[]{:S(2)}) async-start(bf16[32,88,128]{2,1,0:T(8,128)(2,1)} %get-tuple-element.34), calls=%async_computation.3 | async-start | bytes 1441792 | tf_op jit(solution)/shard_map/all_to_all | solution.py:431
  149.1 1.0 slice_bitcast_fusion
  150.5 0.8 fusion.3
  151.5 0.4 fusion.value_part_ref
  151.9 19.4 %all-to-all-done.3.got_ref = bf16[32,88,128]{2,1,0:T(8,128)(2,1)S(1)} async-done(((bf16[32,88,128]{2,1,0:T(8,128)(2,1)}), bf16[32,88,128]{2,1,0:T(8,128)(2,1)S(1)}, u32[]{:S(2)}, u32[]{:S(2)}) %all-to-all-start.3) | async-done | bytes 720928 | tf_op jit(solution)/shard_map/all_to_all | solution.py:431
  171.3 1.5 shard_map.196
  (49 shorter events, 2.5 us)
Async XLA Ops:
  0.6 149.9 %copy-start = (f32[1,1,48,96]{3,2,1,0:T(8,128)S(1)}, f32[1,1,48,96]{3,2,1,0:T(8,128)}, u32[]{:S(2)}) copy-start(f32[1,1,48,96]{3,2,1,0:T(8,128)} %param.27) | copy-start | bytes 55300
  3.2 23.6 %all-to-all-start = ((bf16[32,16,128]{2,1,0:T(8,128)(2,1)}), bf16[32,16,128]{2,1,0:T(8,128)(2,1)S(1)}, u32[]{:S(2)}, u32[]{:S(2)}) async-start(bf16[32,16,128]{2,1,0:T(8,128)(2,1)} %bitcast.4), calls=%async_computation | async-start | bytes 262144 | tf_op jit(solution)/shard_map/all_to_all | solution.py:359
  26.8 37.8 %all-to-all-start.1 = ((bf16[32,16,1024]{2,1,0:T(8,128)(2,1)}), bf16[32,16,1024]{2,1,0:T(8,128)(2,1)S(1)}, u32[]{:S(2)}, u32[]{:S(2)}) async-start(bf16[32,16,1024]{2,1,0:T(8,128)(2,1)} %bitcast.6), calls=%async_computation.1 | async-start | bytes 2097152 | tf_op jit(solution)/shard_map/all_to_all | solution.py:373
  33.4 31.2 %collective-permute-start = (bf16[3,8,128,128]{3,2,1,0:T(8,128)(2,1)}, bf16[3,8,128,128]{3,2,1,0:T(8,128)(2,1)S(1)}, u32[]{:S(2)}, u32[]{:S(2)}) collective-permute-start(bf16[3,8,128,128]{3,2,1,0:T(8,128)(2,1)} %get-tuple-element.30), channel_id=1, source_target_pairs={{0,1},{1,0},{2,3},{3,2},{4,5},{5,4},{6,7},{7,6},{8,9},{9,8},{10,11... | collective-permute-start | bytes 2359304 | tf_op jit(solution)/shard_map/ppermute | solution.py:358
  64.6 5.4 %copy-start.8 = (f32[192,1]{0,1:T(1,128)S(1)}, f32[192,1]{0,1:T(1,128)}, u32[]{:S(2)}) copy-start(f32[192,1]{0,1:T(1,128)} %param.26) | copy-start | bytes 2308
  68.0 4.5 %collective-permute-start.1 = (bf16[512,768]{1,0:T(8,128)(2,1)}, bf16[512,768]{1,0:T(8,128)(2,1)}, u32[]{:S(2)}, u32[]{:S(2)}) collective-permute-start(bf16[512,768]{1,0:T(8,128)(2,1)} %shard_map.192.part_ref), channel_id=1, source_target_pairs={{0,1},{1,0},{2,3},{3,2},{4,5},{5,4},{6,7},{7,6},{8,9},{9,8},{10,11... | collective-permute-start | bytes 2359304 | tf_op jit(solution)/shard_map/ppermute | solution.py:390
  76.7 16.2 %copy-start.7 = (bf16[192,48]{0,1:T(8,128)(2,1)S(1)}, bf16[192,48]{0,1:T(8,128)(2,1)}, u32[]{:S(2)}) copy-start(bf16[192,48]{0,1:T(8,128)(2,1)} %param.24) | copy-start | bytes 55300
  76.7 48.2 %all-to-all-start.2 = ((bf16[256,16,128]{2,1,0:T(8,128)(2,1)}), bf16[256,16,128]{2,1,0:T(8,128)(2,1)S(1)}, u32[]{:S(2)}, u32[]{:S(2)}) async-start(bf16[256,16,128]{2,1,0:T(8,128)(2,1)} %bitcast.82), calls=%async_computation.2 | async-start | bytes 2097152 | tf_op jit(solution)/shard_map/all_to_all | solution.py:406
  93.4 3.4 %copy-start.9 = (bf16[512,512]{1,0:T(8,128)(2,1)S(1)}, bf16[512,512]{1,0:T(8,128)(2,1)}, u32[]{:S(2)}) copy-start(bf16[512,512]{1,0:T(8,128)(2,1)} %get-tuple-element.31) | copy-start | bytes 1572868
  95.0 6.2 %collective-permute-start.3 = (bf16[128,1024]{1,0:T(8,128)(2,1)S(1)}, bf16[128,1024]{1,0:T(8,128)(2,1)S(1)}, u32[]{:S(2)}, u32[]{:S(2)}) collective-permute-start(bf16[128,1024]{1,0:T(8,128)(2,1)S(1)} %slice.56), channel_id=1, source_target_pairs={{0,1},{1,0},{2,3},{3,2},{4,5},{5,4},{6,7},{7,6},{8,9},{9,8},{10,11... | collective-permute-start | bytes 786440 | tf_op jit(solution)/shard_map/ppermute | solution.py:415
  97.6 3.6 %copy-start.5 = (bf16[1024,512]{1,0:T(8,128)(2,1)}, bf16[1024,512]{1,0:T(8,128)(2,1)S(1)}, u32[]{:S(2)}) copy-start(bf16[1024,512]{1,0:T(8,128)(2,1)S(1)} %convolution_convert_fusion) | copy-start | bytes 3145732
  98.6 4.8 %collective-permute-start.2 = (bf16[1024,256]{1,0:T(8,128)(2,1)}, bf16[1024,256]{1,0:T(8,128)(2,1)S(1)}, u32[]{:S(2)}, u32[]{:S(2)}) collective-permute-start(bf16[1024,256]{1,0:T(8,128)(2,1)} %slice.52), channel_id=1, source_target_pairs={{0,1},{1,0},{2,3},{3,2},{4,5},{5,4},{6,7},{7,6},{8,9},{9,8},{10,11... | collective-permute-start | bytes 1572872 | tf_op jit(solution)/shard_map/ppermute | solution.py:411
  104.7 20.4 %copy-start.6 = (bf16[192,128]{1,0:T(8,128)(2,1)S(1)}, bf16[192,128]{1,0:T(8,128)(2,1)}, u32[]{:S(2)}) copy-start(bf16[192,128]{1,0:T(8,128)(2,1)} %grad_hbm.1) | copy-start | bytes 147460
  124.9 18.0 %copy-start.1 = (bf16[96,2048]{1,0:T(8,128)(2,1)S(1)}, bf16[96,2048]{1,0:T(8,128)(2,1)}, u32[]{:S(2)}) copy-start(bf16[96,2048]{1,0:T(8,128)(2,1)} %proj_ref.1) | copy-start | bytes 1179652
  124.9 18.0 %copy-start.2 = (bf16[192,48]{0,1:T(8,128)(2,1)S(1)}, bf16[192,48]{0,1:T(8,128)(2,1)}, u32[]{:S(2)}) copy-start(bf16[192,48]{0,1:T(8,128)(2,1)} %param.23) | copy-start | bytes 55300
  124.9 18.0 %copy-start.3 = (bf16[192,96]{1,0:T(8,128)(2,1)S(1)}, bf16[192,96]{1,0:T(8,128)(2,1)}, u32[]{:S(2)}) copy-start(bf16[192,96]{1,0:T(8,128)(2,1)} %kept_ref.1) | copy-start | bytes 110596
  144.7 26.6 %all-to-all-start.3 = ((bf16[32,88,128]{2,1,0:T(8,128)(2,1)}), bf16[32,88,128]{2,1,0:T(8,128)(2,1)S(1)}, u32[]{:S(2)}, u32[]{:S(2)}) async-start(bf16[32,88,128]{2,1,0:T(8,128)(2,1)} %get-tuple-element.34), calls=%async_computation.3 | async-start | bytes 1441792 | tf_op jit(solution)/shard_map/all_to_all | solution.py:431
  149.1 1.1 copy-start.4

commit v5 on v4

--- a/solution.py
+++ b/solution.py
@@ -153,14 +153,11 @@
     return jnp.concatenate([ref[2, k] for k in range(ref.shape[1])], axis=1)
 
 
-def own_body(rows_ref, grad_ref, mine_hbm, cross_ref, out_ref, mine_ref, sems):
+def own_body(rows_hbm, grad_ref, mine_hbm, cross_ref, out_ref, mine_ref, rows_ref, sems):
     units = mine_ref.shape[3]
     short = grad_ref.shape[0]
-    copies = started(
-        [(mine_hbm.at[part], mine_ref.at[part]) for part in (pl.ds(2, 1), pl.ds(0, 2))], sems
-    )
-    crossed = dot(rows_ref[...], side_by_side((cross_ref,))).astype(out_ref.dtype)
-    out_ref[:, 3 * units : 5 * units] = crossed
+    parts = [(mine_hbm.at[part], mine_ref.at[part]) for part in (pl.ds(2, 1), pl.ds(0, 2))]
+    copies = started([parts[0], (rows_hbm, rows_ref), parts[1]], sems)
     waited(copies[:1])
     downs = jnp.concatenate([lined_up(mine_ref), lined_up(cross_ref)], axis=0)
     back = dot(grad_ref[...], downs, ACROSS).astype(out_ref.dtype)
@@ -169,7 +166,10 @@
         at = 3 * units * k + 2 * units
         out_ref[pl.ds(out_ref.shape[0] - 8, 8), at : at + units] = blank
         out_ref[pl.ds(0, short), at : at + units] = back[:, units * k : units * (k + 1)]
-    waited(copies[1:])
+    waited(copies[1:2])
+    crossed = dot(rows_ref[...], side_by_side((cross_ref,))).astype(out_ref.dtype)
+    out_ref[:, 3 * units : 5 * units] = crossed
+    waited(copies[2:])
     out_ref[:, : 2 * units] = dot(rows_ref[...], side_by_side((mine_ref,))).astype(out_ref.dtype)
 
 
@@ -380,10 +380,11 @@
     rows_own, grad_own = lax.optimization_barrier((rows_own, grad_own))
     (part,) = call(
         own_body,
-        [("v", rows_own), ("v", grad_own), ("h", mine), ("v", cross)],
+        [("h", rows_own), ("v", grad_own), ("h", mine), ("v", cross)],
         [((slots, 6 * units), SWAP_TYPE)],
         scratch=[
-            pltpu.VMEM(mine.shape, BF16), pltpu.SemaphoreType.DMA((2,)),
+            pltpu.VMEM(mine.shape, BF16), pltpu.VMEM((slots, half), BF16),
+            pltpu.SemaphoreType.DMA((3,)),
         ],
         flops=12 * slots * half * units,
     )

time: 174 us -> 173 us (level)
  transfers between devices with their start and end apart: 8 -> 8, of which waited for: 4 -> 4; matrix products, arithmetic and copies ran while one was open for 7% -> 8% of each run, Pallas kernels for 3% -> 3%
where the time goes in v5:
time: 173 us; the launch traced here: 172 us
  waiting for transfers between devices  47.1 us (27%)
  blocking collectives  46.9 us (27%)
  starting transfers between devices  45.8 us (26%)
  Pallas kernels  18 us (10%)
  local copies, waits for them, and re-layouts  6.09 us (4%)
  matrix products  4.35 us (3%)
  other arithmetic  3.18 us (2%)
    all_gather x1, blocking collectives, on_device(): grad_own = lax.all_gather(got_grad, 'y', axis=1, tiled=True)  29.3 us
    all_to_all x1, waiting for transfers between devices, on_device(): got = lax.all_to_all(payload, 'sp', 0, 0, tiled=True)  19.3 us
    all_to_all x1, waiting for transfers between devices, on_device(): pieces = lax.all_to_all(pieces, ('sp', 'y'), 0, 0, tiled=True)  18.8 us
    pallas_call x8, Pallas kernels, call(): pl.pallas_call(body, in_specs=specs, out_specs=places, out_shape=tuple((p...  18 us
    all_gather x1, blocking collectives, on_device(): stream = lax.all_gather(stream_part, TP, axis=1, tiled=True)  17.6 us
    all_to_all x1, starting transfers between devices, on_device(): pieces = lax.all_to_all(pieces, ('sp', 'y'), 0, 0, tiled=True)  15.2 us
    all_to_all x1, starting transfers between devices, on_device(): lax.all_to_all(send_grad.reshape(sp_count, padded, chunk), 'sp', 0, 0, ti...  13.2 us
    all_to_all x1, waiting for transfers between devices, on_device(): lax.all_to_all(send_grad.reshape(sp_count, padded, chunk), 'sp', 0, 0, ti...  7.81 us
  transfers between devices with their start and end apart: 8, of which 4 were waited for; matrix products, arithmetic and copies ran while one was open for 8% of the time, Pallas kernels for 3%

profile of v5, /device:TPU:8, one launch (start us, length us, event | category | flops | bytes accessed | tf_op | source)
XLA Modules:
  0.0 172.5 jit_solution(5424065044851070893)
XLA Ops:
  0.6 2.5 %shard_map.189 = (bf16[192,512]{1,0:T(8,128)(2,1)S(1)}, bf16[512,128]{1,0:T(8,128)(2,1)}) custom-call(s32[2,192]{1,0:T(2,128)} %bitcast.89, f32[2,192]{1,0:T(2,128)} %bitcast.90, bf16[192,128]{1,0:T(8,128)(2,1)} %grad_hbm.1), custom_call_target="tpu_custom_call" | custom-call | tf_op jit(solution)/shard_map/pallas_call | solution.py:35
  3.2 13.2 %all-to-all-start = ((bf16[32,16,128]{2,1,0:T(8,128)(2,1)}), bf16[32,16,128]{2,1,0:T(8,128)(2,1)S(1)}, u32[]{:S(2)}, u32[]{:S(2)}) async-start(bf16[32,16,128]{2,1,0:T(8,128)(2,1)} %bitcast.4), calls=%async_computation | async-start | bytes 262144 | tf_op jit(solution)/shard_map/all_to_all | solution.py:359
  16.3 2.6 %shard_map.190 = bf16[512,1024]{1,0:T(8,128)(2,1)} custom-call(s32[1]{0:T(128)} %bitcast.core_ref, bf16[192,512]{1,0:T(8,128)(2,1)S(1)} %get-tuple-element.23.picker_ref, bf16[192,2048]{1,0:T(8,128)(2,1)} %input_hbm.1, f32[1,192]{1,0:T(1,128)} %bitcast.87), custom_call_target="tpu_custom_call" | custom-call | tf_op jit(solution)/shard_map/pallas_call | solution.py:35
  19.0 7.8 %all-to-all-done = bf16[32,16,128]{2,1,0:T(8,128)(2,1)S(1)} async-done(((bf16[32,16,128]{2,1,0:T(8,128)(2,1)}), bf16[32,16,128]{2,1,0:T(8,128)(2,1)S(1)}, u32[]{:S(2)}, u32[]{:S(2)}) %all-to-all-start) | async-done | bytes 131104 | tf_op jit(solution)/shard_map/all_to_all | solution.py:359
  26.8 4.7 %all-to-all-start.1 = ((bf16[32,16,1024]{2,1,0:T(8,128)(2,1)}), bf16[32,16,1024]{2,1,0:T(8,128)(2,1)}, u32[]{:S(2)}, u32[]{:S(2)}) async-start(bf16[32,16,1024]{2,1,0:T(8,128)(2,1)} %bitcast.6), calls=%async_computation.1 | async-start | bytes 2097152 | tf_op jit(solution)/shard_map/all_to_all | solution.py:373
  31.5 2.7 %shard_map.191 = (bf16[3,8,128,128]{3,2,1,0:T(8,128)(2,1)}, bf16[3,8,128,128]{3,2,1,0:T(8,128)(2,1)}) custom-call(s32[1]{0:T(128)} %bitcast.core_ref, bf16[8,2,128,128]{3,2,1,0:T(8,128)(2,1)} %bitcast.84, bf16[8,2,128,128]{3,2,1,0:T(8,128)(2,1)} %bitcast.85, bf16[128,2048]{1,0:T(8,128)(2,1)} %bitcast.86), custom_call_target="tpu_custom_call" | custom-call | tf_op jit(solution)/shard_map/pallas_call | solution.py:35
  34.2 1.9 %collective-permute-start = (bf16[3,8,128,128]{3,2,1,0:T(8,128)(2,1)}, bf16[3,8,128,128]{3,2,1,0:T(8,128)(2,1)S(1)}, u32[]{:S(2)}, u32[]{:S(2)}) collective-permute-start(bf16[3,8,128,128]{3,2,1,0:T(8,128)(2,1)} %get-tuple-element.30), channel_id=1, source_target_pairs={{0,1},{1,0},{2,3},{3,2},{4,5},{5,4},{6,7},{7,6},{8,9},{9,8},{10,11... | collective-permute-start | bytes 2359304 | tf_op jit(solution)/shard_map/ppermute | solution.py:358
  36.1 29.3 %all_gather.6.grad_ref = bf16[511,1024]{1,0:T(8,128)(2,1)S(1)} all-gather(bf16[511,128]{1,0:T(8,128)(2,1)S(1)} %bitcast.83), channel_id=1, replica_groups=mesh['sp'=32,'y'=8,'c'=2] {'y'}, dimensions={1}, use_global_device_ids=true | all-gather | bytes 1177344 | tf_op jit(solution)/shard_map/all_gather | solution.py:379
  65.4 2.9 %shard_map.192.part_ref = bf16[512,768]{1,0:T(8,128)(2,1)S(1)} custom-call(bf16[512,1024]{1,0:T(8,128)(2,1)} %bitcast.7.rows_hbm, bf16[511,1024]{1,0:T(8,128)(2,1)S(1)} %all_gather.6.grad_ref, bf16[3,8,128,128]{3,2,1,0:T(8,128)(2,1)} %get-tuple-element.29.mine_hbm, bf16[3,8,128,128]{3,2,1,0:T(8,128)(2,1)S(1)} %collective-permute-done.cross_ref), custom_call_target="tpu_custom_call" | custom-call | flops 805306368 | tf_op jit(solution)/shard_map/pallas_call | solution.py:35
  68.3 1.9 %collective-permute-start.1 = (bf16[512,768]{1,0:T(8,128)(2,1)S(1)}, bf16[512,768]{1,0:T(8,128)(2,1)}, u32[]{:S(2)}, u32[]{:S(2)}) collective-permute-start(bf16[512,768]{1,0:T(8,128)(2,1)S(1)} %shard_map.192.part_ref), channel_id=1, source_target_pairs={{0,1},{1,0},{2,3},{3,2},{4,5},{5,4},{6,7},{7,6},{8,9},{9,8},{10,11... | collective-permute-start | bytes 2359304 | tf_op jit(solution)/shard_map/ppermute | solution.py:391
  70.9 0.6 slice.49
  71.5 1.2 collective-permute-done.1.pair_ref
  72.6 3.9 %shard_map.193 = (bf16[511,256]{1,0:T(8,128)(2,1)}, bf16[512,512]{1,0:T(8,128)(2,1)}, bf16[32,8,16,128]{3,2,1,0:T(8,128)(2,1)}) custom-call(bf16[512,768]{1,0:T(8,128)(2,1)S(1)} %shard_map.192.part_ref, bf16[512,768]{1,0:T(8,128)(2,1)} %collective-permute-done.1.pair_ref, bf16[3,8,128,128]{3,2,1,0:T(8,128)(2,1)} %get-tuple-element.29.mine_hbm, ...), custom_call_target="tpu_custom_call" | custom-call | flops 536870912 | tf_op jit(solution)/shard_map/pallas_call | solution.py:35
  76.5 15.2 %all-to-all-start.2 = ((bf16[256,16,128]{2,1,0:T(8,128)(2,1)}), bf16[256,16,128]{2,1,0:T(8,128)(2,1)S(1)}, u32[]{:S(2)}, u32[]{:S(2)}) async-start(bf16[256,16,128]{2,1,0:T(8,128)(2,1)} %bitcast.80), calls=%async_computation.2 | async-start | bytes 2097152 | tf_op jit(solution)/shard_map/all_to_all | solution.py:407
  91.8 1.2 slice_exponential_fusion
  93.2 1.2 fusion.8
  94.5 0.5 convolution_convert_fusion.1
  95.0 1.9 %collective-permute-start.3 = (bf16[128,1024]{1,0:T(8,128)(2,1)S(1)}, bf16[128,1024]{1,0:T(8,128)(2,1)S(1)}, u32[]{:S(2)}, u32[]{:S(2)}) collective-permute-start(bf16[128,1024]{1,0:T(8,128)(2,1)S(1)} %slice.56), channel_id=1, source_target_pairs={{0,1},{1,0},{2,3},{3,2},{4,5},{5,4},{6,7},{7,6},{8,9},{9,8},{10,11... | collective-permute-start | bytes 786440 | tf_op jit(solution)/shard_map/ppermute | solution.py:416
  97.0 2.0 %convolution_convert_fusion = bf16[1024,512]{1,0:T(8,128)(2,1)S(1)} fusion(bf16[512,1024]{1,0:T(8,128)(2,1)} %bitcast.7.rows_hbm, bf16[512,512]{1,0:T(8,128)(2,1)S(1)} %copy-done.11), kind=kOutput, calls=%fused_computation | convolution fusion | flops 537395200 | bytes 2621440 | tf_op jit(solution)/shard_map/dot_general | solution.py:26
  99.0 0.8 slice.52
  99.8 2.6 %collective-permute-start.2 = (bf16[1024,256]{1,0:T(8,128)(2,1)}, bf16[1024,256]{1,0:T(8,128)(2,1)S(1)}, u32[]{:S(2)}, u32[]{:S(2)}) collective-permute-start(bf16[1024,256]{1,0:T(8,128)(2,1)} %slice.52), channel_id=1, source_target_pairs={{0,1},{1,0},{2,3},{3,2},{4,5},{5,4},{6,7},{7,6},{8,9},{9,8},{10,11... | collective-permute-start | bytes 1572872 | tf_op jit(solution)/shard_map/ppermute | solution.py:412
  102.6 0.8 copy.29
  103.4 1.2 broadcast_in_dim_reshape.3
  104.8 1.1 copy.28
  105.8 18.8 %all-to-all-done.2 = bf16[256,16,128]{2,1,0:T(8,128)(2,1)S(1)} async-done(((bf16[256,16,128]{2,1,0:T(8,128)(2,1)}), bf16[256,16,128]{2,1,0:T(8,128)(2,1)S(1)}, u32[]{:S(2)}, u32[]{:S(2)}) %all-to-all-start.2) | async-done | bytes 1048608 | tf_op jit(solution)/shard_map/all_to_all | solution.py:407
  125.0 17.6 %all_gather.7.stream_ref = bf16[192,2048]{1,0:T(8,128)(2,1)S(1)} all-gather(bf16[192,128]{1,0:T(8,128)(2,1)S(1)} %fusion.1), channel_id=1, replica_groups=mesh['sp'=32,'y'=8,'c'=2] {'y','c'}, dimensions={1}, use_global_device_ids=true | all-gather | bytes 835584 | tf_op jit(solution)/shard_map/all_gather | solution.py:422
  142.6 1.8 %shard_map.195 = (bf16[192,96]{1,0:T(8,128)(2,1)S(1)}, bf16[32,88,128]{2,1,0:T(8,128)(2,1)}) custom-call(bf16[192,2048]{1,0:T(8,128)(2,1)S(1)} %all_gather.7.stream_ref, bf16[96,2048]{1,0:T(8,128)(2,1)S(1)} %copy-done.1, bf16[192,96]{1,0:T(8,128)(2,1)S(1)} %copy-done.3, bf16[48,192]{1,0:T(8,128)(2,1)S(1)} %bitcast.74, ...), custom_call_target="tpu_custom_call" | custom-call | flops 150994944 | tf_op jit(solution)/shard_map/pallas_call | solution.py:35
  144.4 4.4 %all-to-all-start.3 = ((bf16[32,88,128]{2,1,0:T(8,128)(2,1)}), bf16[32,88,128]{2,1,0:T(8,128)(2,1)S(1)}, u32[]{:S(2)}, u32[]{:S(2)}) async-start(bf16[32,88,128]{2,1,0:T(8,128)(2,1)} %get-tuple-element.34), calls=%async_computation.3 | async-start | bytes 1441792 | tf_op jit(solution)/shard_map/all_to_all | solution.py:432
  148.9 1.0 slice_bitcast_fusion
  150.3 0.8 fusion.3
  151.7 19.3 %all-to-all-done.3.got_ref = bf16[32,88,128]{2,1,0:T(8,128)(2,1)S(1)} async-done(((bf16[32,88,128]{2,1,0:T(8,128)(2,1)}), bf16[32,88,128]{2,1,0:T(8,128)(2,1)S(1)}, u32[]{:S(2)}, u32[]{:S(2)}) %all-to-all-start.3) | async-done | bytes 720928 | tf_op jit(solution)/shard_map/all_to_all | solution.py:432
  171.0 1.5 shard_map.196
  (53 shorter events, 2.7 us)
Async XLA Ops:
  0.6 149.7 %copy-start = (f32[1,1,48,96]{3,2,1,0:T(8,128)S(1)}, f32[1,1,48,96]{3,2,1,0:T(8,128)}, u32[]{:S(2)}) copy-start(f32[1,1,48,96]{3,2,1,0:T(8,128)} %param.27) | copy-start | bytes 55300
  3.2 23.6 %all-to-all-start = ((bf16[32,16,128]{2,1,0:T(8,128)(2,1)}), bf16[32,16,128]{2,1,0:T(8,128)(2,1)S(1)}, u32[]{:S(2)}, u32[]{:S(2)}) async-start(bf16[32,16,128]{2,1,0:T(8,128)(2,1)} %bitcast.4), calls=%async_computation | async-start | bytes 262144 | tf_op jit(solution)/shard_map/all_to_all | solution.py:359
  26.8 38.6 %all-to-all-start.1 = ((bf16[32,16,1024]{2,1,0:T(8,128)(2,1)}), bf16[32,16,1024]{2,1,0:T(8,128)(2,1)}, u32[]{:S(2)}, u32[]{:S(2)}) async-start(bf16[32,16,1024]{2,1,0:T(8,128)(2,1)} %bitcast.6), calls=%async_computation.1 | async-start | bytes 2097152 | tf_op jit(solution)/shard_map/all_to_all | solution.py:373
  34.2 31.3 %collective-permute-start = (bf16[3,8,128,128]{3,2,1,0:T(8,128)(2,1)}, bf16[3,8,128,128]{3,2,1,0:T(8,128)(2,1)S(1)}, u32[]{:S(2)}, u32[]{:S(2)}) collective-permute-start(bf16[3,8,128,128]{3,2,1,0:T(8,128)(2,1)} %get-tuple-element.30), channel_id=1, source_target_pairs={{0,1},{1,0},{2,3},{3,2},{4,5},{5,4},{6,7},{7,6},{8,9},{9,8},{10,11... | collective-permute-start | bytes 2359304 | tf_op jit(solution)/shard_map/ppermute | solution.py:358
  65.4 4.8 %copy-start.9 = (f32[192,1]{0,1:T(1,128)S(1)}, f32[192,1]{0,1:T(1,128)}, u32[]{:S(2)}) copy-start(f32[192,1]{0,1:T(1,128)} %param.26) | copy-start | bytes 2308
  68.3 4.3 %collective-permute-start.1 = (bf16[512,768]{1,0:T(8,128)(2,1)S(1)}, bf16[512,768]{1,0:T(8,128)(2,1)}, u32[]{:S(2)}, u32[]{:S(2)}) collective-permute-start(bf16[512,768]{1,0:T(8,128)(2,1)S(1)} %shard_map.192.part_ref), channel_id=1, source_target_pairs={{0,1},{1,0},{2,3},{3,2},{4,5},{5,4},{6,7},{7,6},{8,9},{9,8},{10,11... | collective-permute-start | bytes 2359304 | tf_op jit(solution)/shard_map/ppermute | solution.py:391
  76.5 16.6 %copy-start.8 = (bf16[192,48]{0,1:T(8,128)(2,1)S(1)}, bf16[192,48]{0,1:T(8,128)(2,1)}, u32[]{:S(2)}) copy-start(bf16[192,48]{0,1:T(8,128)(2,1)} %param.24) | copy-start | bytes 55300
  76.5 18.0 %copy-start.6 = (bf16[511,256]{1,0:T(8,128)(2,1)S(1)}, bf16[511,256]{1,0:T(8,128)(2,1)}, u32[]{:S(2)}) copy-start(bf16[511,256]{1,0:T(8,128)(2,1)} %get-tuple-element.32) | copy-start | bytes 784900
  76.5 48.1 %all-to-all-start.2 = ((bf16[256,16,128]{2,1,0:T(8,128)(2,1)}), bf16[256,16,128]{2,1,0:T(8,128)(2,1)S(1)}, u32[]{:S(2)}, u32[]{:S(2)}) async-start(bf16[256,16,128]{2,1,0:T(8,128)(2,1)} %bitcast.80), calls=%async_computation.2 | async-start | bytes 2097152 | tf_op jit(solution)/shard_map/all_to_all | solution.py:407
  94.5 2.4 %copy-start.11 = (bf16[512,512]{1,0:T(8,128)(2,1)S(1)}, bf16[512,512]{1,0:T(8,128)(2,1)}, u32[]{:S(2)}) copy-start(bf16[512,512]{1,0:T(8,128)(2,1)} %get-tuple-element.31) | copy-start | bytes 1572868
  95.0 7.3 %collective-permute-start.3 = (bf16[128,1024]{1,0:T(8,128)(2,1)S(1)}, bf16[128,1024]{1,0:T(8,128)(2,1)S(1)}, u32[]{:S(2)}, u32[]{:S(2)}) collective-permute-start(bf16[128,1024]{1,0:T(8,128)(2,1)S(1)} %slice.56), channel_id=1, source_target_pairs={{0,1},{1,0},{2,3},{3,2},{4,5},{5,4},{6,7},{7,6},{8,9},{9,8},{10,11... | collective-permute-start | bytes 786440 | tf_op jit(solution)/shard_map/ppermute | solution.py:416
  99.8 4.8 %collective-permute-start.2 = (bf16[1024,256]{1,0:T(8,128)(2,1)}, bf16[1024,256]{1,0:T(8,128)(2,1)S(1)}, u32[]{:S(2)}, u32[]{:S(2)}) collective-permute-start(bf16[1024,256]{1,0:T(8,128)(2,1)} %slice.52), channel_id=1, source_target_pairs={{0,1},{1,0},{2,3},{3,2},{4,5},{5,4},{6,7},{7,6},{8,9},{9,8},{10,11... | collective-permute-start | bytes 1572872 | tf_op jit(solution)/shard_map/ppermute | solution.py:412
  105.8 18.9 %copy-start.7 = (bf16[192,128]{1,0:T(8,128)(2,1)S(1)}, bf16[192,128]{1,0:T(8,128)(2,1)}, u32[]{:S(2)}) copy-start(bf16[192,128]{1,0:T(8,128)(2,1)} %grad_hbm.1) | copy-start | bytes 147460
  124.6 18.0 %copy-start.1 = (bf16[96,2048]{1,0:T(8,128)(2,1)S(1)}, bf16[96,2048]{1,0:T(8,128)(2,1)}, u32[]{:S(2)}) copy-start(bf16[96,2048]{1,0:T(8,128)(2,1)} %proj_ref.1) | copy-start | bytes 1179652
  124.6 18.0 %copy-start.2 = (bf16[192,48]{0,1:T(8,128)(2,1)S(1)}, bf16[192,48]{0,1:T(8,128)(2,1)}, u32[]{:S(2)}) copy-start(bf16[192,48]{0,1:T(8,128)(2,1)} %param.23) | copy-start | bytes 55300
  124.6 18.0 %copy-start.3 = (bf16[192,96]{1,0:T(8,128)(2,1)S(1)}, bf16[192,96]{1,0:T(8,128)(2,1)}, u32[]{:S(2)}) copy-start(bf16[192,96]{1,0:T(8,128)(2,1)} %kept_ref.1) | copy-start | bytes 110596
  142.6 6.3 %copy-start.5 = (bf16[8,2,128,256]{3,2,1,0:T(8,128)(2,1)S(1)}, bf16[8,2,128,256]{3,2,1,0:T(8,128)(2,1)}, u32[]{:S(2)}) copy-start(bf16[8,2,128,256]{3,2,1,0:T(8,128)(2,1)} %copy.28) | copy-start | bytes 3145732
  144.4 26.6 %all-to-all-start.3 = ((bf16[32,88,128]{2,1,0:T(8,128)(2,1)}), bf16[32,88,128]{2,1,0:T(8,128)(2,1)S(1)}, u32[]{:S(2)}, u32[]{:S(2)}) async-start(bf16[32,88,128]{2,1,0:T(8,128)(2,1)} %get-tuple-element.34), calls=%async_computation.3 | async-start | bytes 1441792 | tf_op jit(solution)/shard_map/all_to_all | solution.py:432
  148.9 1.1 copy-start.4
  148.9 1.1 copy-start.10
